TPU v7x, 32 devices: a whole 2x2x4 slice. The times are simulated.
32 devices in a mesh: sp: 16 (over z, x, core), tp: 2 (over y).
Axes of the slice: x: 2, y: 2, z: 4, core: 2. Of those that a mesh axis runs over, the one named last changes fastest.
Arguments:
- value_rows: bfloat16 [16384, 1024], P('sp', 'tp'), may hold values from -6 to 6
- gate_rows: bfloat16 [16384, 1024], P('sp', 'tp'), may hold values from -6 to 6
- conv_taps: bfloat16 [31, 1024], P(None, 'tp'), may hold values from -1 to 1
- norm_gain: float32 [1024], P('tp'), may hold values from 0.1 to 1.9
- point_weight: bfloat16 [1024, 1024], P(None, 'tp'), may hold values from -0.1875 to 0.1875
- out_grad: bfloat16 [16384, 1024], P('sp', 'tp'), may hold values from -6 to 6
Outputs:
- value_grad: bfloat16 [16384, 1024], P('sp', 'tp')
- gate_grad: bfloat16 [16384, 1024], P('sp', 'tp')
- taps_grad: float32 [31, 1024], P(None, 'tp')
- gain_grad: float32 [1024], P('tp')
- weight_grad: float32 [1024, 1024], P('sp', 'tp')
All inputs are finite; a program needn't handle non-finite values.
Results may differ from a plain program's by a relative error of at most 0.0051.
Values may be sent and summed in bfloat16 or wider, within the bound.
A program may use at most 128 MiB of HBM per device.

v0:
```python
import functools

import jax
import jax.numpy as jnp
from jax import lax
from jax.experimental import pallas as pl
from jax.experimental.pallas import tpu as pltpu
from jax.sharding import PartitionSpec as P

GROUP = 64
EPS = 1e-06
LANE = 128
EDGE = 16
F32, BF16 = jnp.float32, jnp.bfloat16


def sigmoid(x):
    return 0.5 * jnp.tanh(0.5 * x) + 0.5


def divisor(total, *choices):
    for choice in choices:
        if total % choice == 0:
            return choice
    return total


def group_matrix():
    row = lax.broadcasted_iota(jnp.int32, (2 * LANE, LANE), 0)
    col = lax.broadcasted_iota(jnp.int32, (2 * LANE, LANE), 1)
    same = lax.rem(row, LANE) // GROUP == col // GROUP
    return jnp.where(same, 1.0 / GROUP, 0.0).astype(BF16)


def group_mean(x, matrix):
    high = x.astype(BF16)
    low = (x - high.astype(F32)).astype(BF16)
    return jnp.dot(jnp.concatenate([high, low], axis=1), matrix, preferred_element_type=F32)


def near_mean(x, matrix):
    return jnp.dot(x.astype(BF16), matrix[:LANE], preferred_element_type=F32)


def lanes(c):
    return pl.ds(pl.multiple_of(c * LANE, LANE), LANE)


def put_gated(gated, c, v, g, dst, n):
    gated[c, pl.ds(dst, n), :] = (v.astype(F32) * sigmoid(g.astype(F32))).astype(BF16).astype(F32)


def forward_tile(c, taps, gain, gated, unit, inv, normed, matrix):
    kw = taps.shape[1]
    extent = unit.shape[1]
    rows = normed.shape[0]
    cstep = divisor(extent, 96, 32)

    def conv(r, _):
        at = r * cstep
        acc = jnp.zeros((cstep, LANE), F32)
        for k in range(kw):
            acc += taps[c, pl.ds(k, 1), :] * gated[c, pl.ds(at + (k + EDGE - kw // 2), cstep), :]
        unit[c, pl.ds(pl.multiple_of(at, 8), cstep), :] = acc
        return 0

    lax.fori_loop(0, extent // cstep, conv, 0)
    nstep = divisor(extent, 352, 32)

    def norm(r, _):
        at = pl.multiple_of(r * nstep, 8)
        x = unit[c, pl.ds(at, nstep), :]
        centred = x - group_mean(x, matrix)
        rs = lax.rsqrt(near_mean(centred * centred, matrix) + EPS)
        inv[c, pl.ds(at, nstep), :] = rs
        unit[c, pl.ds(at, nstep), :] = centred * rs
        return 0

    lax.fori_loop(0, extent // nstep, norm, 0)
    step = divisor(rows, 256, 32)

    def act(r, _):
        at = pl.multiple_of(r * step, step)
        p = unit[c, pl.ds(pl.multiple_of(at + EDGE, 8), step), :] * gain[:, lanes(c)]
        normed[pl.ds(at, step), lanes(c)] = (p * sigmoid(p)).astype(BF16)
        return 0

    lax.fori_loop(0, rows // step, act, 0)


def act_to_conv(ng, at, n, own, unit, inv, gain, dconv, gain_part, matrix):
    for c in range(unit.shape[0]):
        g = gain[:, c * LANE:(c + 1) * LANE]
        u = unit[c, pl.ds(at, n), :]
        p = u * g
        s = sigmoid(p)
        a = ng[:, c * LANE:(c + 1) * LANE] * s * (1.0 + p * (1.0 - s))
        au = a * u
        if own:
            gain_part[:, c * LANE:(c + 1) * LANE] += jnp.sum(au.reshape(n // 8, 8, LANE), axis=0)
        h = a * g
        hu = au * g
        dconv[c, pl.ds(at, n), :] = inv[c, pl.ds(at, n), :] * (
            h - near_mean(h, matrix) - u * near_mean(hu, matrix))


def taps_tile(c, first, count, dconv, gated, tacc):
    kw = tacc.shape[1]

    def chunk(r, accs):
        at = first + r * 16
        out = []
        d0 = dconv[c, pl.ds(pl.multiple_of(at + EDGE, 8), 8), :]
        d1 = dconv[c, pl.ds(pl.multiple_of(at + EDGE + 8, 8), 8), :]
        for k in range(kw):
            g0 = gated[c, pl.ds(at + (k + 2 * EDGE - kw // 2), 8), :]
            g1 = gated[c, pl.ds(at + (k + 2 * EDGE - kw // 2 + 8), 8), :]
            out.append(accs[k] + (d0 * g0 + d1 * g1))
        return tuple(out)

    accs = lax.fori_loop(0, count // 16, chunk, tuple(tacc[c, k] for k in range(kw)))
    for k in range(kw):
        tacc[c, k] = accs[k]


def fold_taps(c, tacc, gain_part, sums):
    kw = tacc.shape[1]
    for k in range(kw):
        sums[c, pl.ds(k, 1), :] = jnp.sum(tacc[c, k], axis=0, keepdims=True)
    sums[c, pl.ds(kw, 1), :] = jnp.sum(gain_part[:, lanes(c)], axis=0, keepdims=True)


def backward_tile(c, dconv, value, gate, taps, vgrad, ggrad):
    rows = value.shape[0]
    kw = taps.shape[1]
    step = divisor(rows, 64, 32)

    def chunk(r, _):
        at = pl.multiple_of(r * step, step)
        acc = jnp.zeros((step, LANE), F32)
        for k in range(kw):
            acc += taps[c, pl.ds(k, 1), :] * dconv[c, pl.ds(at + (EDGE + kw // 2 - k), step), :]
        s = sigmoid(gate[pl.ds(at, step), lanes(c)].astype(F32))
        v = value[pl.ds(at, step), lanes(c)].astype(F32)
        gs = acc * s
        vgrad[pl.ds(at, step), lanes(c)] = gs.astype(BF16)
        ggrad[pl.ds(at, step), lanes(c)] = (gs * v * (1.0 - s)).astype(BF16)
        return 0

    lax.fori_loop(0, rows // step, chunk, 0)


def loop(lo, hi, body):
    def one(i, _):
        body(i)
        return 0

    lax.fori_loop(lo, hi, one, 0)


def whole_kernel(n, peers, value_in, gate_in, conv_taps, gain, weight_in, grad_in,
                 vgrad_out, ggrad_out, taps_out, gain_out, wout,
                 value, gate, weight, grad, vgrad, ggrad, taps, tacc, lsem, osem,
                 gated, unit, inv, normed, dconv, gain_part, wpart, sums,
                 vhalo, ohalo, others, send1, recv1, send2, recv2, send3, recv3,
                 arecv1, arecv2, asum, arecv3, atotal,
                 vs, vr, os_, or_, gs, gr, ws, wr, ws3, wr3, as_, ar, as3, ar3):
    rows, chans = value.shape
    tiles = chans // LANE
    sp, tp = lax.axis_index("sp"), lax.axis_index("tp")
    group = recv3.shape[0] + 1
    half_tiles = tiles // 2
    b0, b1, zz = lax.rem(sp, 2), lax.rem(sp // 2, 2), sp // 4
    left, right = lax.rem(sp + n - 1, n), lax.rem(sp + 1, n)
    mate0 = sp + 1 - 2 * b0
    mate1 = sp + 2 - 4 * b1

    def zmate(d):
        return lax.rem(sp + 4 * d, n)

    def tmate(j):
        return lax.rem(tp + peers - j, peers)

    def remote(src, dst, s, r, to):
        return pltpu.make_async_remote_copy(
            src_ref=src, dst_ref=dst, send_sem=s, recv_sem=r, device_id=to,
            device_id_type=pl.DeviceIdType.MESH)

    loads = [pltpu.make_async_copy(src, dst, lsem.at[i]) for i, (src, dst) in enumerate(
        ((value_in, value), (gate_in, gate), (grad_in, grad), (weight_in, weight)))]
    for copy in loads:
        copy.start()
    barrier = pltpu.get_barrier_semaphore()
    friends = [(left, tmate(j)) for j in range(peers)] + [(right, tmate(j)) for j in range(peers)]
    friends += [(sp, tmate(j)) for j in range(1, peers)] + [(mate0, tp), (mate1, tp)]
    friends += [(zmate(d), tp) for d in range(1, group)]
    for friend in friends:
        pl.semaphore_signal(barrier, inc=1, device_id=friend, device_id_type=pl.DeviceIdType.MESH)
    pl.semaphore_wait(barrier, len(friends))

    wide = 2 * EDGE
    pending = []
    halos = []
    for side, (start, to) in enumerate(((rows - wide, right), (0, left))):
        for i, ref in enumerate((value_in, gate_in)):
            halos.append(remote(ref.at[pl.ds(start, wide)], vhalo.at[side, i], vs.at[side, i], vr.at[side, i], (to, tp)))
    ohalos = []
    for side, (start, to) in enumerate(((rows - EDGE, right), (0, left))):
        for j in range(peers):
            ohalos.append(remote(grad_in.at[pl.ds(start, EDGE)], ohalo.at[side, j], os_.at[side, j], or_.at[side, j], (to, tmate(j))))
    for copy in halos + ohalos:
        copy.start()
    pending += halos + ohalos
    chunks = gs.shape[1]
    step = rows // chunks

    def gather(j, r):
        at = pl.ds(pl.multiple_of(r * step, step), step)
        return remote(grad_in.at[at], others.at[j - 1, at], gs.at[j - 1, r], gr.at[j - 1, r], (sp, tmate(j)))

    for r in range(chunks):
        for j in range(1, peers):
            copy = gather(j, r)
            copy.start()
            pending.append(copy)

    matrix = group_matrix()
    for c in range(tiles):
        taps[c] = conv_taps[:, c * LANE:(c + 1) * LANE].astype(F32)
    gain_part[...] = jnp.zeros_like(gain_part)
    tacc[...] = jnp.zeros_like(tacc)
    loads[0].wait()
    loads[1].wait()
    gstep = divisor(rows, 256, 32)

    def own_gated(c):
        def chunk(r):
            at = pl.multiple_of(r * gstep, gstep)
            put_gated(gated, c, value[pl.ds(at, gstep), lanes(c)], gate[pl.ds(at, gstep), lanes(c)],
                      pl.multiple_of(at + wide, 8), gstep)

        loop(0, rows // gstep, chunk)

    loop(0, tiles, own_gated)
    for copy in halos:
        copy.wait_recv()
    inside = ((sp > 0).astype(F32), (sp < n - 1).astype(F32))

    def front(c):
        for side, dst in ((0, 0), (1, rows + wide)):
            put_gated(gated, c, vhalo[side, 0, :, lanes(c)].astype(F32) * inside[side],
                      vhalo[side, 1, :, lanes(c)], dst, wide)
        forward_tile(c, taps, gain, gated, unit, inv, normed, matrix)

    loop(0, tiles, front)

    def owner(j):
        return pl.ds(pl.multiple_of(lax.rem(tp + j, peers) * chans, chans), chans)

    per = wpart.shape[1]
    piece = max(divisor(chans, 256, 128), per)

    def weight_part(j):
        def cols(q):
            at = pl.ds(pl.multiple_of(q * piece, piece), piece)
            lhs = grad[:, at] if j == 0 else others[j - 1, :, at]
            out = lax.dot_general(lhs, normed[...], (((0,), (0,)), ((), ())), preferred_element_type=F32)
            base = lax.rem(tp + j, peers) * (chans // per) + q * (piece // per)
            wpart[pl.ds(base, piece // per)] = out.reshape(piece // per, per, chans)

        loop(0, chans // piece, cols)

    pairs, quads = n // 2 // peers, n // 4 // peers
    span = group // peers

    def half1(j):
        at = pl.ds(lax.rem(tp + j, peers) * pairs, pairs)
        return remote(send1.at[at], recv1.at[at], ws.at[0, j], wr.at[0, j], (mate0, tp))

    def half2(j):
        at = pl.ds(lax.rem(tp + j, peers) * quads, quads)
        return remote(send2.at[at], recv2.at[at], ws.at[1, j], wr.at[1, j], (mate1, tp))

    def start1(j):
        first = lax.rem(tp + j, peers) * pairs

        def cast(i):
            send1[first + i] = wpart[2 * (first + i) + 1 - b0].astype(BF16)

        loop(0, pairs, cast)
        half1(j).start()

    def start2(j):
        first = lax.rem(tp + j, peers) * quads
        half1(j).wait_recv()

        def cast(i):
            other, mine = 2 * (first + i) + 1 - b1, 2 * (first + i) + b1
            send2[first + i] = (wpart[2 * other + b0] + recv1[other].astype(F32)).astype(BF16)
            wpart[2 * mine + b0] = wpart[2 * mine + b0] + recv1[mine].astype(F32)

        loop(0, quads, cast)
        half2(j).start()

    def total2(z):
        return wpart[4 * z + 2 * b1 + b0] + recv2[z].astype(F32)

    def final_copy(slot):
        return remote(send3.at[slot], recv3.at[slot], ws3.at[slot], wr3.at[slot],
                      (lax.rem(sp + 4 * (slot + 1), n), tp))

    def start3(j):
        half2(j).wait_recv()

        def one(i):
            z = lax.rem(tp + j, peers) * span + i
            d = lax.rem(z + group - zz, group)

            @pl.when(d != 0)
            def _():
                send3[d - 1] = total2(z).astype(BF16)
                final_copy(d - 1).start()

        loop(0, span, one)

    def await_chunk(r):
        for j in range(1, peers):
            gather(j, r).wait_recv()

    def middle(r):
        at = pl.multiple_of(r * step, step)
        ng = jnp.dot(grad[pl.ds(at, step), :], weight[owner(0), :], preferred_element_type=F32)
        for j in range(1, peers):
            ng += jnp.dot(others[j - 1, pl.ds(at, step), :], weight[owner(j), :], preferred_element_type=F32)
        act_to_conv(ng, pl.multiple_of(at + EDGE, 8), step, True, unit, inv, gain, dconv, gain_part, matrix)

    def taps_chunk(r):
        loop(0, tiles, lambda c: taps_tile(c, pl.multiple_of(r * step, step), step, dconv, gated, tacc))

    def both(r):
        await_chunk(r)
        middle(r)
        taps_chunk(r)

    def put_out(c):
        backward_tile(c, dconv, value, gate, taps, vgrad, ggrad)
        for copy in out_copies(c):
            copy.start()

    def out_copies(c):
        return (pltpu.make_async_copy(vgrad.at[:, lanes(c)], vgrad_out.at[:, lanes(c)], osem.at[0, c]),
                pltpu.make_async_copy(ggrad.at[:, lanes(c)], ggrad_out.at[:, lanes(c)], osem.at[1, c]))

    loads[2].wait()
    weight_part(0)
    start1(0)
    loads[3].wait()
    for copy in ohalos:
        copy.wait_recv()
    for side, at in ((0, 0), (1, rows + EDGE)):
        ng = sum(jnp.dot(ohalo[side, j], weight[owner(j), :], preferred_element_type=F32) for j in range(peers))
        act_to_conv(ng * inside[side], at, EDGE, False, unit, inv, gain, dconv, gain_part, matrix)
    start2(0)
    loop(0, chunks - 1, both)
    start3(0)
    await_chunk(chunks - 1)
    for j in range(1, peers):
        weight_part(j)
        start1(j)
    middle(chunks - 1)
    for j in range(1, peers):
        start2(j)
    taps_chunk(chunks - 1)
    loop(0, tiles, lambda c: fold_taps(c, tacc, gain_part, sums))

    acopy1 = remote(sums.at[pl.ds((1 - b0) * half_tiles, half_tiles)], arecv1, as_.at[0], ar.at[0], (mate0, tp))
    acopy1.start()
    quarter = max(tiles // 4, 1)
    loop(0, quarter, put_out)
    acopy1.wait_recv()
    asum[0] = sums[pl.ds(b0 * half_tiles, half_tiles)] + arecv1[...]
    acopy2 = remote(asum.at[0], arecv2, as_.at[1], ar.at[1], (mate1, tp))
    acopy2.start()
    loop(quarter, 2 * quarter, put_out)
    acopy2.wait_recv()
    asum[1] = asum[0] + arecv2[...]
    acopies3 = []
    for d in range(1, group):
        copy = remote(asum.at[1], arecv3.at[zz], as3.at[d - 1], ar3.at[d - 1], (zmate(d), tp))
        copy.start()
        acopies3.append(copy)
    for j in range(1, peers):
        start3(j)
    loop(2 * quarter, tiles, put_out)
    for d in range(1, group):
        peer = lax.rem(zz + group - d, group)
        remote(asum.at[1], arecv3.at[peer], as3.at[d - 1], ar3.at[d - 1], (zmate(d), tp)).wait_recv()
    arecv3[zz] = asum[1]
    total = arecv3[0]
    for z in range(1, group):
        total += arecv3[z]
    atotal[b0] = total
    acopy4 = remote(atotal.at[b0], atotal.at[b0], as_.at[2], ar.at[2], (mate0, tp))
    acopy4.start()
    final = total2(zz)
    for d in range(1, group):
        final_copy(d - 1).wait_recv()
        final += recv3[d - 1].astype(F32)
    wout[...] = final
    remote(atotal.at[1 - b0], atotal.at[1 - b0], as_.at[2], ar.at[2], (mate0, tp)).wait_recv()
    kw = tacc.shape[1]
    for c in range(tiles):
        tot = atotal[c // half_tiles, c % half_tiles]
        taps_out[:, c * LANE:(c + 1) * LANE] = tot[:kw]
        gain_out[:, c * LANE:(c + 1) * LANE] = tot[kw:]
    for copy in pending + [acopy1, acopy2, acopy4] + acopies3:
        copy.wait_send()
    for j in range(peers):
        half1(j).wait_send()
        half2(j).wait_send()
    for d in range(1, group):
        final_copy(d - 1).wait_send()

    def drain(c):
        for copy in out_copies(c):
            copy.wait()

    loop(0, tiles, drain)


def finish_kernel(parts, *refs):
    count = len(parts)
    sources, targets, held = refs[:count], refs[count:2 * count], refs[2 * count:3 * count]
    isem, osem = refs[3 * count:]
    incoming, outgoing = [], []
    slot = 0
    for src, dst, buf, pieces in zip(sources, targets, held, parts):
        size = src.shape[0] // pieces
        for p in range(pieces):
            at = pl.ds(p * size, size)
            incoming.append(pltpu.make_async_copy(src.at[at], buf.at[at], isem.at[slot]))
            outgoing.append(pltpu.make_async_copy(buf.at[at], dst.at[at], osem.at[slot]))
            slot += 1
    for copy in incoming:
        copy.start()
    for copy, after in zip(incoming, outgoing):
        copy.wait()
        after.start()
    for copy in outgoing:
        copy.wait()


def finish(*arrays):
    parts = [4 if a.shape[0] % 128 == 0 else 1 for a in arrays]
    sems = pltpu.SemaphoreType.DMA((sum(parts),))
    return pl.pallas_call(
        functools.partial(finish_kernel, parts),
        out_shape=[jax.ShapeDtypeStruct(a.shape, a.dtype) for a in arrays],
        in_specs=[pl.BlockSpec(memory_space=pl.ANY)] * len(arrays),
        out_specs=[pl.BlockSpec(memory_space=pl.ANY)] * len(arrays),
        scratch_shapes=[pltpu.VMEM(a.shape, a.dtype) for a in arrays] + [sems, sems],
        compiler_params=pltpu.CompilerParams(vmem_limit_bytes=60 * 1024 * 1024),
    )(*arrays)


def per_device(value, gate, conv_taps, norm_gain, point_weight, out_grad):
    rows, chans = value.shape
    kw = conv_taps.shape[0]
    tiles = chans // LANE
    n, peers = lax.axis_size("sp"), lax.axis_size("tp")
    extent = rows + 2 * EDGE
    full = point_weight.shape[0]
    per = full // n
    group = n // 4
    gain = norm_gain.reshape(1, chans)
    args = (value, gate, conv_taps, gain, point_weight, out_grad)
    half = (tiles // 2, kw + 1, LANE)
    vmem, dma = pltpu.VMEM, pltpu.SemaphoreType.DMA
    chunks = 4
    outs = [((rows, chans), BF16), ((rows, chans), BF16), ((kw, chans), F32), ((1, chans), F32), ((per, chans), F32)]
    vgrad, ggrad, taps_grad, gain_grad, wgrad = pl.pallas_call(
        functools.partial(whole_kernel, n, peers),
        out_shape=[jax.ShapeDtypeStruct(s, d) for s, d in outs],
        in_specs=[pl.BlockSpec(memory_space=m) for m in (pl.ANY, pl.ANY, vmem, vmem, pl.ANY, pl.ANY)],
        out_specs=[pl.BlockSpec(memory_space=m) for m in (pl.ANY, pl.ANY, vmem, vmem, vmem)],
        scratch_shapes=[
            vmem((rows, chans), BF16), vmem((rows, chans), BF16), vmem((full, chans), BF16), vmem((rows, chans), BF16),
            vmem((rows, chans), BF16), vmem((rows, chans), BF16),
            vmem((tiles, kw, LANE), F32),
            vmem((tiles, kw, 8, LANE), F32),
            dma((4,)), dma((2, tiles)),
            vmem((tiles, rows + 4 * EDGE, LANE), F32),
            vmem((tiles, extent, LANE), F32),
            vmem((tiles, extent, LANE), F32),
            vmem((rows, chans), BF16),
            vmem((tiles, extent, LANE), F32),
            vmem((8, chans), F32),
            vmem((n, per, chans), F32),
            vmem((tiles, kw + 1, LANE), F32),
            vmem((2, 2, 2 * EDGE, chans), BF16),
            vmem((2, peers, EDGE, chans), BF16),
            vmem((peers - 1, rows, chans), BF16),
            vmem((n // 2, per, chans), BF16),
            vmem((n // 2, per, chans), BF16),
            vmem((n // 4, per, chans), BF16),
            vmem((n // 4, per, chans), BF16),
            vmem((group - 1, per, chans), BF16),
            vmem((group - 1, per, chans), BF16),
            vmem(half, F32),
            vmem(half, F32),
            vmem((2,) + half, F32),
            vmem((group,) + half, F32),
            vmem((2,) + half, F32),
            dma((2, 2)), dma((2, 2)), dma((2, peers)), dma((2, peers)),
            dma((peers - 1, chunks)), dma((peers - 1, chunks)),
            dma((2, peers)), dma((2, peers)), dma((group - 1,)), dma((group - 1,)),
            dma((3,)), dma((3,)), dma((group - 1,)), dma((group - 1,)),
        ],
        compiler_params=pltpu.CompilerParams(
            collective_id=0, has_side_effects=True, vmem_limit_bytes=56 * 1024 * 1024),
    )(*args)
    vgrad, ggrad, taps_grad, gain_grad, wgrad = finish(vgrad, ggrad, taps_grad, gain_grad, wgrad)
    return vgrad, ggrad, taps_grad, gain_grad.reshape(chans), wgrad


def solution(mesh):
    return jax.shard_map(
        per_device,
        mesh=mesh,
        in_specs=(P("sp", "tp"), P("sp", "tp"), P(None, "tp"), P("tp"), P(None, "tp"), P("sp", "tp")),
        out_specs=(P("sp", "tp"), P("sp", "tp"), P(None, "tp"), P("tp"), P("sp", "tp")),
        check_vma=False,
    )
```

profile of v0, /device:TPU:24, one launch (start us, length us, event | category | flops | bytes accessed | tf_op | source)
XLA Modules:
  0.0 52.0 jit_solution(3691588222118122038)
XLA Ops:
  0.6 48.9 %shard_map.101 = (bf16[1024,512]{1,0:T(8,128)(2,1)}, bf16[1024,512]{1,0:T(8,128)(2,1)}, f32[31,512]{1,0:T(8,128)}, f32[1,512]{1,0:T(1,128)}, f32[64,512]{1,0:T(8,128)}) custom-call(bf16[1024,512]{1,0:T(8,128)(2,1)} %value_in.1, bf16[1024,512]{1,0:T(8,128)(2,1)} %gate_in.1, bf16[31,512]{1,0:T(8,128)(2,1)} %conv_taps.1, f32[1,512]{1,0:T(1,128)} %bitcast.2, ...), custom_call_target="tpu_custom_call" | custom-call | tf_op jit(solution)/shard_map/pallas_call | solution.py:481
  49.5 2.5 %shard_map.102 = (bf16[1024,512]{1,0:T(8,128)(2,1)}, bf16[1024,512]{1,0:T(8,128)(2,1)}, f32[31,512]{1,0:T(8,128)}, f32[1,512]{1,0:T(1,128)}, f32[64,512]{1,0:T(8,128)}) custom-call(bf16[1024,512]{1,0:T(8,128)(2,1)} %get-tuple-element.15.refs_0_, bf16[1024,512]{1,0:T(8,128)(2,1)} %get-tuple-element.16.refs_1_, f32[31,512]{1,0:T(8,128)} %get-tuple-element.17.refs_2_, ...), custom_call_target="tpu_custom_call" | custom-call | tf_op jit(solution)/shard_map/pallas_call | solution.py:456
where the time goes:
time: 52.2 us; the launch traced here: 52 us
  Pallas kernels  51.4 us (98%)
  between operations  0.64 us (1%)
    pallas_call x1, Pallas kernels, per_device(): pl.pallas_call(functools.partial(whole_kernel, n, peers), out_shape=[jax....  48.9 us
    pallas_call x1, Pallas kernels, finish(): pl.pallas_call(functools.partial(finish_kernel, parts), out_shape=[jax.Sh...  2.51 us

commit v1 on v0

v1 whole, which is shorter than its diff:
```python
import functools

import jax
import jax.numpy as jnp
from jax import lax
from jax.experimental import pallas as pl
from jax.experimental.pallas import tpu as pltpu
from jax.sharding import PartitionSpec as P

GROUP = 64
EPS = 1e-06
LANE = 128
EDGE = 16
WIDE = 2 * EDGE
SEG = 16
TAU = 8
CHUNK = SEG * TAU
UNIT = 2 * LANE
F32, BF16 = jnp.float32, jnp.bfloat16


def sigmoid(x):
    return 0.5 * jnp.tanh(0.5 * x) + 0.5


def divisor(total, *choices):
    for choice in choices:
        if total % choice == 0:
            return choice
    return total


def group_matrix():
    row = lax.broadcasted_iota(jnp.int32, (2 * LANE, LANE), 0)
    col = lax.broadcasted_iota(jnp.int32, (2 * LANE, LANE), 1)
    same = lax.rem(row, LANE) // GROUP == col // GROUP
    return jnp.where(same, 1.0 / GROUP, 0.0).astype(BF16)


def group_mean(x, matrix):
    high = x.astype(BF16)
    low = (x - high.astype(F32)).astype(BF16)
    return jnp.dot(jnp.concatenate([high, low], axis=1), matrix, preferred_element_type=F32)


def near_mean(x, matrix):
    return jnp.dot(x.astype(BF16), matrix[:LANE], preferred_element_type=F32)


def lanes(c):
    return pl.ds(pl.multiple_of(c * LANE, LANE), LANE)


def loop(lo, hi, body):
    def one(i, _):
        body(i)
        return 0

    lax.fori_loop(lo, hi, one, 0)


def put_gated(gated, c, v, g, dst, n):
    gated[c, pl.ds(dst, n), :] = (v.astype(F32) * sigmoid(g.astype(F32))).astype(BF16).astype(F32)


def spread(src, c, low, high, stride):
    half = SEG // 2
    return jnp.concatenate([src[c, pl.ds(low, half, stride=stride), :],
                            src[c, pl.ds(high, half, stride=stride), :]], axis=0).astype(BF16)


def products(pairs):
    sums = [None] * len(pairs)
    for step in zip(*pairs):
        for a, (x, y) in enumerate(step):
            p = x().astype(F32) * y().astype(F32)
            sums[a] = p if sums[a] is None else sums[a] + p
    return sums


def conv_block(kw, source, tapb, c, taus, reverse, put):
    width = min(4, taus)
    for first in range(0, taus, width):
        pairs = []
        for a in range(width):
            tau = first + a
            pairs.append([
                ((lambda j=(tau + kw - 1 - k if reverse else tau + k): source(j)), (lambda k=k: tapb[c, k]))
                for k in range(kw)])
        for a, total in enumerate(products(pairs)):
            put(first + a, total)


def act_to_conv(ng, at, n, own, unit, inv, gain, dconv, gain_part, matrix):
    for c in range(unit.shape[0]):
        g = gain[:, c * LANE:(c + 1) * LANE]
        u = unit[c, pl.ds(at, n), :]
        p = u * g
        s = sigmoid(p)
        a = ng[:, c * LANE:(c + 1) * LANE] * s * (1.0 + p * (1.0 - s))
        au = a * u
        if own:
            gain_part[:, c * LANE:(c + 1) * LANE] += jnp.sum(au.reshape(n // 8, 8, LANE), axis=0)
        h = a * g
        hu = au * g
        dconv[c, pl.ds(at, n), :] = inv[c, pl.ds(at, n), :] * (
            h - near_mean(h, matrix) - u * near_mean(hu, matrix))


def whole_kernel(n, peers, value_in, gate_in, taps_in, gain_in, weight_in, grad_in,
                 vgrad_out, ggrad_out, taps_out, gain_out, wout,
                 value, gate, weight, grad, taps_raw, gain, vgrad, ggrad, taps, tapb, tacc, lsem, osem,
                 gated, shifted, edges, unit, inv, normed, dconv, dshift, dpack, grow, ngacc,
                 gain_part, wpart, sums,
                 vhalo, ohalo, others, send1, recv1, send2, recv2, send3, recv3,
                 arecv1, asend2, arecv2, atotal, asend3, arecv3,
                 vs, vr, os_, or_, gs, gr, ws, wr, ws3, wr3, as_, ar, as3, ar3):
    rows, chans = value.shape
    tiles = chans // LANE
    kw = taps.shape[1]
    sp, tp = lax.axis_index("sp"), lax.axis_index("tp")
    group = recv3.shape[0] + 1
    half_tiles = tiles // 2
    b0, b1, zz = lax.rem(sp, 2), lax.rem(sp // 2, 2), sp // 4
    has_left, has_right = sp > 0, sp < n - 1
    left, right = lax.rem(sp + n - 1, n), lax.rem(sp + 1, n)
    mate0 = sp + 1 - 2 * b0
    mate1 = sp + 2 - 4 * b1
    chunks = rows // CHUNK
    owned = chans // UNIT
    units = (peers - 1) * owned

    def zmate(d):
        return lax.rem(sp + 4 * d, n)

    def tmate(j):
        return lax.rem(tp + peers - j, peers)

    def remote(src, dst, s, r, to):
        return pltpu.make_async_remote_copy(
            src_ref=src, dst_ref=dst, send_sem=s, recv_sem=r, device_id=to,
            device_id_type=pl.DeviceIdType.MESH)

    barrier = pltpu.get_barrier_semaphore()

    def hello(friend):
        pl.semaphore_signal(barrier, inc=1, device_id=friend, device_id_type=pl.DeviceIdType.MESH)

    friends = [(sp, tmate(j)) for j in range(1, peers)] + [(mate0, tp), (mate1, tp)]
    friends += [(zmate(d), tp) for d in range(1, group)]
    for friend in friends:
        hello(friend)

    @pl.when(has_left)
    def _():
        for j in range(peers):
            hello((left, tmate(j)))

    @pl.when(has_right)
    def _():
        for j in range(peers):
            hello((right, tmate(j)))

    loads = [pltpu.make_async_copy(src, dst, lsem.at[i]) for i, (src, dst) in enumerate(
        ((grad_in, grad), (value_in, value), (gate_in, gate), (taps_in, taps_raw), (gain_in, gain), (weight_in, weight)))]
    for copy in loads:
        copy.start()
    loads[0].wait()
    pl.semaphore_wait(barrier, len(friends) + peers * (has_left.astype(jnp.int32) + has_right.astype(jnp.int32)))

    halos = [[remote(ref.at[pl.ds(start, WIDE)], vhalo.at[side, i], vs.at[side, i], vr.at[side, i], (to, tp))
              for i, ref in enumerate((value_in, gate_in))]
             for side, (start, to) in enumerate(((rows - WIDE, right), (0, left)))]
    ohalos = [[remote(grad.at[pl.ds(start, EDGE)], ohalo.at[side, j], os_.at[side, j], or_.at[side, j], (to, tmate(j)))
               for j in range(peers)]
              for side, (start, to) in enumerate(((rows - EDGE, right), (0, left)))]
    sends = (has_right, has_left)
    arrives = (has_left, has_right)

    def unit_lane(p):
        p = lax.rem(p, owned)
        return pl.multiple_of(jnp.where(2 * tp < peers, owned - 1 - p, p) * UNIT, UNIT)

    def gather(p, r):
        j = p // owned + 1
        at = (pl.ds(pl.multiple_of(r * CHUNK, CHUNK), CHUNK), pl.ds(unit_lane(p), UNIT))
        return remote(grad.at[at], others.at[(j - 1,) + at], gs.at[p, r], gr.at[p, r], (sp, tmate(j)))

    def start_halos(copies):
        for side in range(2):
            @pl.when(sends[side])
            def _(side=side):
                for copy in copies[side]:
                    copy.start()

    def unit_lane_from(p):
        j = p // owned + 1
        sender = lax.rem(tp + j, peers)
        q = lax.rem(p, owned)
        return pl.multiple_of(jnp.where(2 * sender < peers, owned - 1 - q, q) * UNIT, UNIT)

    start_halos(halos)
    for p in range(units):
        for r in range(chunks):
            gather(p, r).start()
        if p == 0:
            start_halos(ohalos)

    matrix = group_matrix()
    loads[3].wait()
    for c in range(tiles):
        taps[c] = taps_raw[:, c * LANE:(c + 1) * LANE].astype(F32)

    def widen(c):
        for k in range(kw):
            tapb[c, k] = jnp.broadcast_to(taps[c, pl.ds(k, 1), :], (SEG, LANE)).astype(BF16)

    loop(0, tiles, widen)
    gain_part[...] = jnp.zeros_like(gain_part)
    tacc[...] = jnp.zeros_like(tacc)
    loads[1].wait()
    loads[2].wait()
    gstep = divisor(rows, 256, 32)

    def own_gated(c):
        def chunk(r):
            at = pl.multiple_of(r * gstep, gstep)
            put_gated(gated, c, value[pl.ds(at, gstep), lanes(c)], gate[pl.ds(at, gstep), lanes(c)],
                      pl.multiple_of(at + WIDE, 8), gstep)

        loop(0, rows // gstep, chunk)

    loop(0, tiles, own_gated)

    def put_halos():
        for side, dst in ((0, 0), (1, rows + WIDE)):
            @pl.when(arrives[side])
            def _(side=side, dst=dst):
                for copy in halos[side]:
                    copy.wait_recv()

                def one(c):
                    put_gated(gated, c, vhalo[side, 0, :, lanes(c)], vhalo[side, 1, :, lanes(c)], dst, WIDE)

                loop(0, tiles, one)

            @pl.when(jnp.logical_not(arrives[side]))
            def _(dst=dst):
                for c in range(tiles):
                    gated[c, pl.ds(dst, WIDE), :] = jnp.zeros((WIDE, LANE), F32)

    def forward(i):
        r = lax.rem(i + 1, chunks)
        base = r * CHUNK

        @pl.when(i == chunks - 2)
        def _():
            put_halos()

        def tile(c):
            for j in range(TAU + kw - 1):
                low = base + (j + WIDE - kw // 2)
                shifted[c, r, j] = spread(gated, c, low, low + TAU * (SEG // 2), TAU)

            def put(tau, total):
                for h in range(2):
                    start = base + (EDGE + tau + h * TAU * (SEG // 2))
                    unit[c, pl.ds(start, SEG // 2, stride=TAU), :] = total[h * (SEG // 2):(h + 1) * (SEG // 2)]

            conv_block(kw, lambda j: shifted[c, r, j], tapb, c, TAU, False, put)

        loop(0, tiles, tile)

    loop(0, chunks, forward)

    def forward_edges(c):
        for j in range(2 + kw - 1):
            edges[j] = spread(gated, c, EDGE - kw // 2 + j, rows + WIDE - kw // 2 + j, 2)

        def put(tau, total):
            for h, start in ((0, tau), (1, rows + EDGE + tau)):
                unit[c, pl.ds(start, SEG // 2, stride=2), :] = total[h * (SEG // 2):(h + 1) * (SEG // 2)]

        conv_block(kw, lambda j: edges[j], tapb, c, 2, False, put)

    loop(0, tiles, forward_edges)
    loads[4].wait()

    def norm_rows(c, at, count):
        x = unit[c, pl.ds(at, count), :]
        centred = x - group_mean(x, matrix)
        rs = lax.rsqrt(near_mean(centred * centred, matrix) + EPS)
        inv[c, pl.ds(at, count), :] = rs
        u = centred * rs
        unit[c, pl.ds(at, count), :] = u
        return u

    nstep = divisor(rows, 256, 32)

    def norm(c):
        def chunk(r):
            at = pl.multiple_of(r * nstep, nstep)
            p = norm_rows(c, pl.multiple_of(at + EDGE, 8), nstep) * gain[:, lanes(c)]
            normed[pl.ds(at, nstep), lanes(c)] = (p * sigmoid(p)).astype(BF16)

        loop(0, rows // nstep, chunk)
        norm_rows(c, 0, EDGE)
        norm_rows(c, rows + EDGE, EDGE)

    loop(0, tiles, norm)

    def owner(j):
        return lax.rem(tp + j, peers)

    per = wpart.shape[1]
    span = UNIT // per

    def unit_of(j, p):
        lane = unit_lane_from((j - 1) * owned + p) if j else pl.multiple_of(p * UNIT, UNIT)
        return lane, (owner(j) * chans + lane) // per

    def weight_part(j, p, first, count, add):
        lane, base = unit_of(j, p)
        at = (pl.ds(first, count), pl.ds(lane, UNIT))
        lhs = others[(j - 1,) + at] if j else grad[at]
        out = lax.dot_general(lhs, normed[pl.ds(first, count), :], (((0,), (0,)), ((), ())), preferred_element_type=F32)
        out = out.reshape(span, per, chans)
        wpart[pl.ds(base, span)] = wpart[pl.ds(base, span)] + out if add else out

    pairs, quads, far = span // 2, span // 4, span // 4

    def half1(j, p):
        at = pl.ds(unit_of(j, p)[1] // 2, pairs)
        k = j * owned + p
        return remote(send1.at[at], recv1.at[at], ws.at[0, k], wr.at[0, k], (mate0, tp))

    def half2(j, p):
        at = pl.ds(unit_of(j, p)[1] // 4, quads)
        k = j * owned + p
        return remote(send2.at[at], recv2.at[at], ws.at[1, k], wr.at[1, k], (mate1, tp))

    def start1(j, p):
        first = unit_of(j, p)[1] // 2

        def cast(i):
            send1[first + i] = wpart[2 * (first + i) + 1 - b0].astype(BF16)

        loop(0, pairs, cast)
        half1(j, p).start()

    def start2(j, p):
        first = unit_of(j, p)[1] // 4
        half1(j, p).wait_recv()

        def cast(i):
            other, mine = 2 * (first + i) + 1 - b1, 2 * (first + i) + b1
            send2[first + i] = (wpart[2 * other + b0] + recv1[other].astype(F32)).astype(BF16)
            wpart[2 * mine + b0] = wpart[2 * mine + b0] + recv1[mine].astype(F32)

        loop(0, quads, cast)
        half2(j, p).start()

    def total2(z):
        return wpart[4 * z + 2 * b1 + b0] + recv2[z].astype(F32)

    def final_copy(slot):
        return remote(send3.at[slot], recv3.at[slot], ws3.at[slot], wr3.at[slot],
                      (lax.rem(sp + 4 * (slot + 1), n), tp))

    def start3(j, p):
        half2(j, p).wait_recv()
        first = unit_of(j, p)[1] // 4

        def one(i):
            z = first + i
            d = lax.rem(z + group - zz, group)

            @pl.when(d != 0)
            def _():
                send3[d - 1] = total2(z).astype(BF16)
                final_copy(d - 1).start()

        loop(0, far, one)

    def weight_rows(j, lane):
        return pl.ds(pl.multiple_of(owner(j) * chans + lane, UNIT), UNIT)

    def partial_ng(r):
        at = pl.ds(pl.multiple_of(r * nstep, nstep), nstep)
        total = jnp.dot(grad[at, :], weight[pl.ds(pl.multiple_of(owner(0) * chans, UNIT), chans), :],
                        preferred_element_type=F32)
        for p in range(units - 1):
            lane = unit_lane_from(p)
            j = p // owned + 1
            total += jnp.dot(others[j - 1, at, pl.ds(lane, UNIT)], weight[weight_rows(j, lane), :],
                             preferred_element_type=F32)
        ngacc[at, :] = total

    last_lane = unit_lane_from(units - 1)

    def middle(r):
        gather(units - 1, r).wait_recv()
        at = pl.ds(pl.multiple_of(r * CHUNK, CHUNK), CHUNK)
        ng = ngacc[at, :] + jnp.dot(others[peers - 2, at, pl.ds(last_lane, UNIT)], weight[weight_rows(peers - 1, last_lane), :],
                                    preferred_element_type=F32)
        act_to_conv(ng, pl.multiple_of(r * CHUNK + EDGE, 8), CHUNK, True, unit, inv, gain, dconv, gain_part, matrix)

    def taps_chunk(r):
        def tile(c):
            for tau in range(TAU):
                low = r * CHUNK + (EDGE + tau)
                dpack[c, tau] = spread(dconv, c, low, low + TAU * (SEG // 2), TAU)
            for k0 in range(0, kw, 4):
                ks = range(k0, min(k0 + 4, kw))
                pairs_ = [[((lambda j=tau + k: shifted[c, r, j]), (lambda tau=tau: dpack[c, tau])) for tau in range(TAU)]
                          for k in ks]
                for k, total in zip(ks, products(pairs_)):
                    tacc[c, k] += total[:SEG // 2] + total[SEG // 2:]

        loop(0, tiles, tile)

    def finalize(r):
        middle(r)
        taps_chunk(r)

    def fold_taps(c):
        for k in range(kw):
            sums[c, pl.ds(k, 1), :] = jnp.sum(tacc[c, k], axis=0, keepdims=True)
        sums[c, pl.ds(kw, 1), :] = jnp.sum(gain_part[:, lanes(c)], axis=0, keepdims=True)

    def edge_conv():
        for side, at in ((0, 0), (1, rows + EDGE)):
            @pl.when(arrives[side])
            def _(side=side, at=at):
                for copy in ohalos[side]:
                    copy.wait_recv()
                ng = sum(jnp.dot(ohalo[side, j], weight[pl.ds(pl.multiple_of(owner(j) * chans, UNIT), chans), :],
                                 preferred_element_type=F32) for j in range(peers))
                act_to_conv(ng, at, EDGE, False, unit, inv, gain, dconv, gain_part, matrix)

            @pl.when(jnp.logical_not(arrives[side]))
            def _(at=at):
                for c in range(tiles):
                    dconv[c, pl.ds(at, EDGE), :] = jnp.zeros((EDGE, LANE), F32)

    def backward(r):
        def tile(c):
            base = r * CHUNK
            for j in range(TAU + kw - 1):
                low = base + (EDGE - kw // 2 + j)
                dshift[j] = spread(dconv, c, low, low + TAU * (SEG // 2), TAU)

            def put(tau, total):
                for h in range(2):
                    grow[c, pl.ds(tau + h * TAU * (SEG // 2), SEG // 2, stride=TAU), :] = (
                        total[h * (SEG // 2):(h + 1) * (SEG // 2)])

            conv_block(kw, lambda j: dshift[j], tapb, c, TAU, True, put)
            at = pl.ds(pl.multiple_of(base, CHUNK), CHUNK)
            s = sigmoid(gate[at, lanes(c)].astype(F32))
            v = value[at, lanes(c)].astype(F32)
            out = grow[c] * s
            vgrad[at, lanes(c)] = out.astype(BF16)
            ggrad[at, lanes(c)] = (out * v * (1.0 - s)).astype(BF16)

        loop(0, tiles, tile)
        for copy in out_copies(r):
            copy.start()

    def out_copies(r):
        at = pl.ds(pl.multiple_of(r * CHUNK, CHUNK), CHUNK)
        return (pltpu.make_async_copy(vgrad.at[at], vgrad_out.at[at], osem.at[0, r]),
                pltpu.make_async_copy(ggrad.at[at], ggrad_out.at[at], osem.at[1, r]))

    for p in range(owned):
        weight_part(0, p, 0, rows, False)
        start1(0, p)
    for p in range(owned):
        start2(0, p)
    loads[5].wait()
    for p in range(units - 1):
        for r in range(chunks):
            gather(p, r).wait_recv()
        weight_part(p // owned + 1, p % owned, 0, rows, False)
        start1(p // owned + 1, p % owned)
    loop(0, rows // nstep, partial_ng)
    for p in range(owned):
        start3(0, p)
    edge_conv()
    for p in range(units - 1):
        start2(p // owned + 1, p % owned)
    lj, lp = peers - 1, owned - 1
    loop(0, chunks - 2, finalize)
    for p in range(units - 1):
        start3(p // owned + 1, p % owned)
    weight_part(lj, lp, 0, rows - 2 * CHUNK, False)
    finalize(chunks - 2)
    middle(chunks - 1)
    weight_part(lj, lp, rows - 2 * CHUNK, 2 * CHUNK, True)
    start1(lj, lp)
    taps_chunk(chunks - 1)
    loop(0, tiles, fold_taps)

    acopy1 = remote(sums.at[pl.ds((1 - b0) * half_tiles, half_tiles)], arecv1, as_.at[0], ar.at[0], (mate0, tp))
    acopy1.start()
    start2(lj, lp)
    acopy1.wait_recv()
    mine = (sums[pl.ds(b0 * half_tiles, half_tiles)] + arecv1[...]).astype(BF16)
    asend2[...] = mine
    acopy2 = remote(asend2, arecv2, as_.at[1], ar.at[1], (mate1, tp))
    acopy2.start()
    backward(0)
    backward(1)
    acopy2.wait_recv()
    asend3[...] = (asend2[...].astype(F32) + arecv2[...].astype(F32)).astype(BF16)
    acopies3 = []
    for d in range(1, group):
        copy = remote(asend3, arecv3.at[zz], as3.at[d - 1], ar3.at[d - 1], (zmate(d), tp))
        copy.start()
        acopies3.append(copy)
    loop(2, 4, backward)
    start3(lj, lp)
    loop(4, chunks, backward)
    arecv3[zz] = asend3[...]
    for d in range(1, group):
        peer = lax.rem(zz + group - d, group)
        remote(asend3, arecv3.at[peer], as3.at[d - 1], ar3.at[d - 1], (zmate(d), tp)).wait_recv()
    total = arecv3[0].astype(F32)
    for z in range(1, group):
        total += arecv3[z].astype(F32)
    atotal[b0] = total
    acopy4 = remote(atotal.at[b0], atotal.at[b0], as_.at[2], ar.at[2], (mate0, tp))
    acopy4.start()
    final = total2(zz)
    for d in range(1, group):
        final_copy(d - 1).wait_recv()
        final += recv3[d - 1].astype(F32)
    wout[...] = final
    remote(atotal.at[1 - b0], atotal.at[1 - b0], as_.at[2], ar.at[2], (mate0, tp)).wait_recv()
    for c in range(tiles):
        tot = atotal[c // half_tiles, c % half_tiles]
        taps_out[:, c * LANE:(c + 1) * LANE] = tot[:kw]
        gain_out[:, c * LANE:(c + 1) * LANE] = tot[kw:]
    for side in range(2):
        @pl.when(sends[side])
        def _(side=side):
            for copy in halos[side] + ohalos[side]:
                copy.wait_send()
    for copy in [acopy1, acopy2, acopy4] + acopies3:
        copy.wait_send()
    for p in range(units):
        for r in range(chunks):
            gather(p, r).wait_send()
    for j in range(peers):
        for p in range(owned):
            half1(j, p).wait_send()
            half2(j, p).wait_send()
    for d in range(1, group):
        final_copy(d - 1).wait_send()

    def drain(r):
        for copy in out_copies(r):
            copy.wait()

    loop(0, chunks, drain)


def finish_kernel(parts, *refs):
    count = len(parts)
    sources, targets, held = refs[:count], refs[count:2 * count], refs[2 * count:3 * count]
    isem, osem = refs[3 * count:]
    incoming, outgoing = [], []
    slot = 0
    for src, dst, buf, pieces in zip(sources, targets, held, parts):
        size = src.shape[0] // pieces
        for p in range(pieces):
            at = pl.ds(p * size, size)
            incoming.append(pltpu.make_async_copy(src.at[at], buf.at[at], isem.at[slot]))
            outgoing.append(pltpu.make_async_copy(buf.at[at], dst.at[at], osem.at[slot]))
            slot += 1
    for copy in incoming:
        copy.start()
    for copy, after in zip(incoming, outgoing):
        copy.wait()
        after.start()
    for copy in outgoing:
        copy.wait()


def finish(*arrays):
    parts = [4 if a.shape[0] % 128 == 0 else 1 for a in arrays]
    sems = pltpu.SemaphoreType.DMA((sum(parts),))
    return pl.pallas_call(
        functools.partial(finish_kernel, parts),
        out_shape=[jax.ShapeDtypeStruct(a.shape, a.dtype) for a in arrays],
        in_specs=[pl.BlockSpec(memory_space=pl.ANY)] * len(arrays),
        out_specs=[pl.BlockSpec(memory_space=pl.ANY)] * len(arrays),
        scratch_shapes=[pltpu.VMEM(a.shape, a.dtype) for a in arrays] + [sems, sems],
        compiler_params=pltpu.CompilerParams(vmem_limit_bytes=60 * 1024 * 1024),
    )(*arrays)


def per_device(value, gate, conv_taps, norm_gain, point_weight, out_grad):
    rows, chans = value.shape
    kw = conv_taps.shape[0]
    tiles = chans // LANE
    n, peers = lax.axis_size("sp"), lax.axis_size("tp")
    extent = rows + WIDE
    full = point_weight.shape[0]
    per = full // n
    group = n // 4
    chunks = rows // CHUNK
    owned = chans // UNIT
    units = (peers - 1) * owned
    gain = norm_gain.reshape(1, chans)
    args = (value, gate, conv_taps, gain, point_weight, out_grad)
    half = (tiles // 2, kw + 1, LANE)
    vmem, dma = pltpu.VMEM, pltpu.SemaphoreType.DMA
    block = (SEG, LANE)
    outs = [((rows, chans), BF16), ((rows, chans), BF16), ((kw, chans), F32), ((1, chans), F32), ((per, chans), F32)]
    vgrad, ggrad, taps_grad, gain_grad, wgrad = pl.pallas_call(
        functools.partial(whole_kernel, n, peers),
        out_shape=[jax.ShapeDtypeStruct(s, d) for s, d in outs],
        in_specs=[pl.BlockSpec(memory_space=pl.ANY)] * 6,
        out_specs=[pl.BlockSpec(memory_space=m) for m in (pl.ANY, pl.ANY, vmem, vmem, vmem)],
        scratch_shapes=[
            vmem((rows, chans), BF16), vmem((rows, chans), BF16), vmem((full, chans), BF16), vmem((rows, chans), BF16),
            vmem((kw, chans), BF16), vmem((1, chans), F32),
            vmem((rows, chans), BF16), vmem((rows, chans), BF16),
            vmem((tiles, kw, LANE), F32),
            vmem((tiles, kw) + block, BF16),
            vmem((tiles, kw, 8, LANE), F32),
            dma((6,)), dma((2, chunks)),
            vmem((tiles, rows + 4 * EDGE, LANE), F32),
            vmem((tiles, chunks, TAU + kw - 1) + block, BF16),
            vmem((kw + 1,) + block, BF16),
            vmem((tiles, extent, LANE), F32),
            vmem((tiles, extent, LANE), F32),
            vmem((rows, chans), BF16),
            vmem((tiles, extent, LANE), F32),
            vmem((TAU + kw - 1,) + block, BF16),
            vmem((tiles, TAU) + block, BF16),
            vmem((tiles, CHUNK, LANE), F32),
            vmem((rows, chans), F32),
            vmem((8, chans), F32),
            vmem((n, per, chans), F32),
            vmem((tiles, kw + 1, LANE), F32),
            vmem((2, 2, WIDE, chans), BF16),
            vmem((2, peers, EDGE, chans), BF16),
            vmem((peers - 1, rows, chans), BF16),
            vmem((n // 2, per, chans), BF16),
            vmem((n // 2, per, chans), BF16),
            vmem((n // 4, per, chans), BF16),
            vmem((n // 4, per, chans), BF16),
            vmem((group - 1, per, chans), BF16),
            vmem((group - 1, per, chans), BF16),
            vmem(half, F32),
            vmem(half, BF16),
            vmem(half, BF16),
            vmem((2,) + half, F32),
            vmem(half, BF16),
            vmem((group,) + half, BF16),
            dma((2, 2)), dma((2, 2)), dma((2, peers)), dma((2, peers)),
            dma((units, chunks)), dma((units, chunks)),
            dma((2, peers * owned)), dma((2, peers * owned)), dma((group - 1,)), dma((group - 1,)),
            dma((3,)), dma((3,)), dma((group - 1,)), dma((group - 1,)),
        ],
        compiler_params=pltpu.CompilerParams(
            collective_id=0, has_side_effects=True, vmem_limit_bytes=60 * 1024 * 1024),
    )(*args)
    vgrad, ggrad, taps_grad, gain_grad, wgrad = finish(vgrad, ggrad, taps_grad, gain_grad, wgrad)
    return vgrad, ggrad, taps_grad, gain_grad.reshape(chans), wgrad


def solution(mesh):
    return jax.shard_map(
        per_device,
        mesh=mesh,
        in_specs=(P("sp", "tp"), P("sp", "tp"), P(None, "tp"), P("tp"), P(None, "tp"), P("sp", "tp")),
        out_specs=(P("sp", "tp"), P("sp", "tp"), P(None, "tp"), P("tp"), P("sp", "tp")),
        check_vma=False,
    )
```

time: 52.2 us -> 46.3 us (0.89)
  the two profiles are of different devices: /device:TPU:24 before, /device:TPU:5 now
where the time goes in v1:
time: 46.3 us; the launch traced here: 46.1 us
  Pallas kernels  45.5 us (98%)
  between operations  0.64 us (1%)
    pallas_call x1, Pallas kernels, per_device(): pl.pallas_call(functools.partial(whole_kernel, n, peers), out_shape=[jax....  43 us
    pallas_call x1, Pallas kernels, finish(): pl.pallas_call(functools.partial(finish_kernel, parts), out_shape=[jax.Sh...  2.51 us

profile of v1, /device:TPU:5, one launch (start us, length us, event | category | flops | bytes accessed | tf_op | source)
XLA Modules:
  0.0 46.1 jit_solution(15413534984180723669)
XLA Ops:
  0.6 43.0 %shard_map.101 = (bf16[1024,512]{1,0:T(8,128)(2,1)}, bf16[1024,512]{1,0:T(8,128)(2,1)}, f32[31,512]{1,0:T(8,128)}, f32[1,512]{1,0:T(1,128)}, f32[64,512]{1,0:T(8,128)}) custom-call(bf16[1024,512]{1,0:T(8,128)(2,1)} %value_in.1, bf16[1024,512]{1,0:T(8,128)(2,1)} %gate_in.1, bf16[31,512]{1,0:T(8,128)(2,1)} %taps_in.1, f32[1,512]{1,0:T(1,128)} %bitcast.2, ...), custom_call_target="tpu_custom_call" | custom-call | tf_op jit(solution)/shard_map/pallas_call | solution.py:621
  43.6 2.5 %shard_map.102 = (bf16[1024,512]{1,0:T(8,128)(2,1)}, bf16[1024,512]{1,0:T(8,128)(2,1)}, f32[31,512]{1,0:T(8,128)}, f32[1,512]{1,0:T(1,128)}, f32[64,512]{1,0:T(8,128)}) custom-call(bf16[1024,512]{1,0:T(8,128)(2,1)} %get-tuple-element.15.refs_0_, bf16[1024,512]{1,0:T(8,128)(2,1)} %get-tuple-element.16.refs_1_, f32[31,512]{1,0:T(8,128)} %get-tuple-element.17.refs_2_, ...), custom_call_target="tpu_custom_call" | custom-call | tf_op jit(solution)/shard_map/pallas_call | solution.py:593

commit v2 on v1

--- a/solution.py
+++ b/solution.py
@@ -108,19 +108,18 @@
 
 
 def whole_kernel(n, peers, value_in, gate_in, taps_in, gain_in, weight_in, grad_in,
-                 vgrad_out, ggrad_out, taps_out, gain_out, wout,
-                 value, gate, weight, grad, taps_raw, gain, vgrad, ggrad, taps, tapb, tacc, lsem, osem,
+                 vgrad, ggrad, taps_out, gain_out, wout,
+                 value, gate, weight, grad, taps_raw, gain, taps, tapb, tacc, lsem,
                  gated, shifted, edges, unit, inv, normed, dconv, dshift, dpack, grow, ngacc,
                  gain_part, wpart, sums,
                  vhalo, ohalo, others, send1, recv1, send2, recv2, send3, recv3,
-                 arecv1, asend2, arecv2, atotal, asend3, arecv3,
+                 asend, arecv, atotal, zsend, zrecv,
                  vs, vr, os_, or_, gs, gr, ws, wr, ws3, wr3, as_, ar, as3, ar3):
     rows, chans = value.shape
     tiles = chans // LANE
     kw = taps.shape[1]
     sp, tp = lax.axis_index("sp"), lax.axis_index("tp")
     group = recv3.shape[0] + 1
-    half_tiles = tiles // 2
     b0, b1, zz = lax.rem(sp, 2), lax.rem(sp // 2, 2), sp // 4
     has_left, has_right = sp > 0, sp < n - 1
     left, right = lax.rem(sp + n - 1, n), lax.rem(sp + 1, n)
@@ -130,6 +129,11 @@
     owned = chans // UNIT
     units = (peers - 1) * owned
 
+    quarter = lax.rem(sp, 4)
+
+    def plane(d):
+        return sp - quarter + lax.rem(quarter + d, 4)
+
     def zmate(d):
         return lax.rem(sp + 4 * d, n)
 
@@ -146,7 +150,7 @@
     def hello(friend):
         pl.semaphore_signal(barrier, inc=1, device_id=friend, device_id_type=pl.DeviceIdType.MESH)
 
-    friends = [(sp, tmate(j)) for j in range(1, peers)] + [(mate0, tp), (mate1, tp)]
+    friends = [(sp, tmate(j)) for j in range(1, peers)] + [(plane(d), tp) for d in range(1, 4)]
     friends += [(zmate(d), tp) for d in range(1, group)]
     for friend in friends:
         hello(friend)
@@ -163,15 +167,15 @@
 
     loads = [pltpu.make_async_copy(src, dst, lsem.at[i]) for i, (src, dst) in enumerate(
         ((grad_in, grad), (value_in, value), (gate_in, gate), (taps_in, taps_raw), (gain_in, gain), (weight_in, weight)))]
+    loads = loads[1:3] + loads[:1] + loads[3:]
     for copy in loads:
         copy.start()
-    loads[0].wait()
     pl.semaphore_wait(barrier, len(friends) + peers * (has_left.astype(jnp.int32) + has_right.astype(jnp.int32)))
 
     halos = [[remote(ref.at[pl.ds(start, WIDE)], vhalo.at[side, i], vs.at[side, i], vr.at[side, i], (to, tp))
               for i, ref in enumerate((value_in, gate_in))]
              for side, (start, to) in enumerate(((rows - WIDE, right), (0, left)))]
-    ohalos = [[remote(grad.at[pl.ds(start, EDGE)], ohalo.at[side, j], os_.at[side, j], or_.at[side, j], (to, tmate(j)))
+    ohalos = [[remote(grad_in.at[pl.ds(start, EDGE)], ohalo.at[side, j], os_.at[side, j], or_.at[side, j], (to, tmate(j)))
                for j in range(peers)]
               for side, (start, to) in enumerate(((rows - EDGE, right), (0, left)))]
     sends = (has_right, has_left)
@@ -179,12 +183,12 @@
 
     def unit_lane(p):
         p = lax.rem(p, owned)
-        return pl.multiple_of(jnp.where(2 * tp < peers, owned - 1 - p, p) * UNIT, UNIT)
+        return pl.multiple_of(jnp.where(2 * tp < peers, p, owned - 1 - p) * UNIT, UNIT)
 
     def gather(p, r):
         j = p // owned + 1
         at = (pl.ds(pl.multiple_of(r * CHUNK, CHUNK), CHUNK), pl.ds(unit_lane(p), UNIT))
-        return remote(grad.at[at], others.at[(j - 1,) + at], gs.at[p, r], gr.at[p, r], (sp, tmate(j)))
+        return remote(grad_in.at[at], others.at[(j - 1,) + at], gs.at[p, r], gr.at[p, r], (sp, tmate(j)))
 
     def start_halos(copies):
         for side in range(2):
@@ -197,14 +201,13 @@
         j = p // owned + 1
         sender = lax.rem(tp + j, peers)
         q = lax.rem(p, owned)
-        return pl.multiple_of(jnp.where(2 * sender < peers, owned - 1 - q, q) * UNIT, UNIT)
+        return pl.multiple_of(jnp.where(2 * sender < peers, q, owned - 1 - q) * UNIT, UNIT)
 
     start_halos(halos)
     for p in range(units):
         for r in range(chunks):
             gather(p, r).start()
-        if p == 0:
-            start_halos(ohalos)
+    start_halos(ohalos)
 
     matrix = group_matrix()
     loads[3].wait()
@@ -218,8 +221,8 @@
     loop(0, tiles, widen)
     gain_part[...] = jnp.zeros_like(gain_part)
     tacc[...] = jnp.zeros_like(tacc)
+    loads[0].wait()
     loads[1].wait()
-    loads[2].wait()
     gstep = divisor(rows, 256, 32)
 
     def own_gated(c):
@@ -286,28 +289,28 @@
     loop(0, tiles, forward_edges)
     loads[4].wait()
 
-    def norm_rows(c, at, count):
-        x = unit[c, pl.ds(at, count), :]
-        centred = x - group_mean(x, matrix)
-        rs = lax.rsqrt(near_mean(centred * centred, matrix) + EPS)
-        inv[c, pl.ds(at, count), :] = rs
-        u = centred * rs
-        unit[c, pl.ds(at, count), :] = u
-        return u
-
+    def norm_rows(at, count):
+        xs = [unit[c, pl.ds(at, count), :] for c in range(tiles)]
+        centred = [x - group_mean(x, matrix) for x in xs]
+        out = []
+        for c in range(tiles):
+            rs = lax.rsqrt(near_mean(centred[c] * centred[c], matrix) + EPS)
+            inv[c, pl.ds(at, count), :] = rs
+            u = centred[c] * rs
+            unit[c, pl.ds(at, count), :] = u
+            out.append(u)
+        return out
+
+    def norm(r):
+        at = pl.multiple_of(r * CHUNK, CHUNK)
+        for c, u in enumerate(norm_rows(pl.multiple_of(at + EDGE, 8), CHUNK)):
+            p = u * gain[:, c * LANE:(c + 1) * LANE]
+            normed[pl.ds(at, CHUNK), c * LANE:(c + 1) * LANE] = (p * sigmoid(p)).astype(BF16)
+
+    loop(0, chunks, norm)
+    norm_rows(0, EDGE)
+    norm_rows(rows + EDGE, EDGE)
     nstep = divisor(rows, 256, 32)
-
-    def norm(c):
-        def chunk(r):
-            at = pl.multiple_of(r * nstep, nstep)
-            p = norm_rows(c, pl.multiple_of(at + EDGE, 8), nstep) * gain[:, lanes(c)]
-            normed[pl.ds(at, nstep), lanes(c)] = (p * sigmoid(p)).astype(BF16)
-
-        loop(0, rows // nstep, chunk)
-        norm_rows(c, 0, EDGE)
-        norm_rows(c, rows + EDGE, EDGE)
-
-    loop(0, tiles, norm)
 
     def owner(j):
         return lax.rem(tp + j, peers)
@@ -385,21 +388,24 @@
     def weight_rows(j, lane):
         return pl.ds(pl.multiple_of(owner(j) * chans + lane, UNIT), UNIT)
 
-    def partial_ng(r):
+    def own_ng(r):
         at = pl.ds(pl.multiple_of(r * nstep, nstep), nstep)
-        total = jnp.dot(grad[at, :], weight[pl.ds(pl.multiple_of(owner(0) * chans, UNIT), chans), :],
-                        preferred_element_type=F32)
-        for p in range(units - 1):
+        ngacc[at, :] = jnp.dot(grad[at, :], weight[pl.ds(pl.multiple_of(owner(0) * chans, UNIT), chans), :],
+                               preferred_element_type=F32)
+
+    def unit_ng(p):
+        def add(r):
+            at = pl.ds(pl.multiple_of(r * nstep, nstep), nstep)
             lane = unit_lane_from(p)
             j = p // owned + 1
-            total += jnp.dot(others[j - 1, at, pl.ds(lane, UNIT)], weight[weight_rows(j, lane), :],
-                             preferred_element_type=F32)
-        ngacc[at, :] = total
+            ngacc[at, :] += jnp.dot(others[j - 1, at, pl.ds(lane, UNIT)], weight[weight_rows(j, lane), :],
+                                    preferred_element_type=F32)
+
+        loop(0, rows // nstep, add)
 
     last_lane = unit_lane_from(units - 1)
 
     def middle(r):
-        gather(units - 1, r).wait_recv()
         at = pl.ds(pl.multiple_of(r * CHUNK, CHUNK), CHUNK)
         ng = ngacc[at, :] + jnp.dot(others[peers - 2, at, pl.ds(last_lane, UNIT)], weight[weight_rows(peers - 1, last_lane), :],
                                     preferred_element_type=F32)
@@ -420,6 +426,7 @@
         loop(0, tiles, tile)
 
     def finalize(r):
+        gather(units - 1, r).wait_recv()
         middle(r)
         taps_chunk(r)
 
@@ -464,81 +471,93 @@
             ggrad[at, lanes(c)] = (out * v * (1.0 - s)).astype(BF16)
 
         loop(0, tiles, tile)
-        for copy in out_copies(r):
-            copy.start()
-
-    def out_copies(r):
-        at = pl.ds(pl.multiple_of(r * CHUNK, CHUNK), CHUNK)
-        return (pltpu.make_async_copy(vgrad.at[at], vgrad_out.at[at], osem.at[0, r]),
-                pltpu.make_async_copy(ggrad.at[at], ggrad_out.at[at], osem.at[1, r]))
-
+
+    part = (kw + 1) // 4
+
+    def slot(d):
+        return lax.rem(quarter + d, 4)
+
+    def gather_sums(d):
+        return remote(asend.at[slot(d)], arecv.at[d - 1], as_.at[0, d - 1], ar.at[0, d - 1], (plane(d), tp))
+
+    def share(d):
+        return remote(atotal.at[quarter], atotal.at[quarter], as_.at[1, d - 1], ar.at[1, d - 1], (plane(d), tp))
+
+    def shared_from(d):
+        return remote(atotal.at[slot(4 - d)], atotal.at[slot(4 - d)], as_.at[1, d - 1], ar.at[1, d - 1], (plane(d), tp))
+
+    loads[2].wait()
     for p in range(owned):
         weight_part(0, p, 0, rows, False)
         start1(0, p)
+    loads[5].wait()
+    loop(0, rows // nstep, own_ng)
     for p in range(owned):
         start2(0, p)
-    loads[5].wait()
     for p in range(units - 1):
         for r in range(chunks):
             gather(p, r).wait_recv()
         weight_part(p // owned + 1, p % owned, 0, rows, False)
         start1(p // owned + 1, p % owned)
-    loop(0, rows // nstep, partial_ng)
+        unit_ng(p)
     for p in range(owned):
         start3(0, p)
-    edge_conv()
     for p in range(units - 1):
         start2(p // owned + 1, p % owned)
     lj, lp = peers - 1, owned - 1
-    loop(0, chunks - 2, finalize)
+    loop(0, 3, finalize)
     for p in range(units - 1):
         start3(p // owned + 1, p % owned)
+    loop(3, chunks - 2, finalize)
     weight_part(lj, lp, 0, rows - 2 * CHUNK, False)
     finalize(chunks - 2)
-    middle(chunks - 1)
+    gather(units - 1, chunks - 1).wait_recv()
     weight_part(lj, lp, rows - 2 * CHUNK, 2 * CHUNK, True)
     start1(lj, lp)
+    middle(chunks - 1)
     taps_chunk(chunks - 1)
     loop(0, tiles, fold_taps)
-
-    acopy1 = remote(sums.at[pl.ds((1 - b0) * half_tiles, half_tiles)], arecv1, as_.at[0], ar.at[0], (mate0, tp))
-    acopy1.start()
+    for q in range(4):
+        asend[q] = sums[:, q * part:(q + 1) * part, :].astype(BF16)
+    for d in range(1, 4):
+        gather_sums(d).start()
     start2(lj, lp)
-    acopy1.wait_recv()
-    mine = (sums[pl.ds(b0 * half_tiles, half_tiles)] + arecv1[...]).astype(BF16)
-    asend2[...] = mine
-    acopy2 = remote(asend2, arecv2, as_.at[1], ar.at[1], (mate1, tp))
-    acopy2.start()
-    backward(0)
-    backward(1)
-    acopy2.wait_recv()
-    asend3[...] = (asend2[...].astype(F32) + arecv2[...].astype(F32)).astype(BF16)
+    loop(1, 5, backward)
+    for d in range(1, 4):
+        gather_sums(d).wait_recv()
+    mine = sums[:, pl.ds(pl.multiple_of(quarter * part, part), part), :]
+    for d in range(3):
+        mine += arecv[d].astype(F32)
+    zsend[...] = mine.astype(BF16)
     acopies3 = []
     for d in range(1, group):
-        copy = remote(asend3, arecv3.at[zz], as3.at[d - 1], ar3.at[d - 1], (zmate(d), tp))
+        copy = remote(zsend, zrecv.at[zz], as3.at[d - 1], ar3.at[d - 1], (zmate(d), tp))
         copy.start()
         acopies3.append(copy)
-    loop(2, 4, backward)
+    edge_conv()
+    backward(0)
+    backward(chunks - 1)
     start3(lj, lp)
-    loop(4, chunks, backward)
-    arecv3[zz] = asend3[...]
+    loop(5, chunks - 1, backward)
+    zrecv[zz] = zsend[...]
     for d in range(1, group):
         peer = lax.rem(zz + group - d, group)
-        remote(asend3, arecv3.at[peer], as3.at[d - 1], ar3.at[d - 1], (zmate(d), tp)).wait_recv()
-    total = arecv3[0].astype(F32)
+        remote(zsend, zrecv.at[peer], as3.at[d - 1], ar3.at[d - 1], (zmate(d), tp)).wait_recv()
+    total = zrecv[0].astype(F32)
     for z in range(1, group):
-        total += arecv3[z].astype(F32)
-    atotal[b0] = total
-    acopy4 = remote(atotal.at[b0], atotal.at[b0], as_.at[2], ar.at[2], (mate0, tp))
-    acopy4.start()
+        total += zrecv[z].astype(F32)
+    atotal[quarter] = total
+    for d in range(1, 4):
+        share(d).start()
     final = total2(zz)
     for d in range(1, group):
         final_copy(d - 1).wait_recv()
         final += recv3[d - 1].astype(F32)
     wout[...] = final
-    remote(atotal.at[1 - b0], atotal.at[1 - b0], as_.at[2], ar.at[2], (mate0, tp)).wait_recv()
+    for d in range(1, 4):
+        shared_from(d).wait_recv()
     for c in range(tiles):
-        tot = atotal[c // half_tiles, c % half_tiles]
+        tot = jnp.concatenate([atotal[q, c] for q in range(4)], axis=0)
         taps_out[:, c * LANE:(c + 1) * LANE] = tot[:kw]
         gain_out[:, c * LANE:(c + 1) * LANE] = tot[kw:]
     for side in range(2):
@@ -546,7 +565,7 @@
         def _(side=side):
             for copy in halos[side] + ohalos[side]:
                 copy.wait_send()
-    for copy in [acopy1, acopy2, acopy4] + acopies3:
+    for copy in acopies3 + [gather_sums(d) for d in range(1, 4)] + [share(d) for d in range(1, 4)]:
         copy.wait_send()
     for p in range(units):
         for r in range(chunks):
@@ -558,46 +577,31 @@
     for d in range(1, group):
         final_copy(d - 1).wait_send()
 
-    def drain(r):
-        for copy in out_copies(r):
-            copy.wait()
-
-    loop(0, chunks, drain)
-
 
 def finish_kernel(parts, *refs):
     count = len(parts)
-    sources, targets, held = refs[:count], refs[count:2 * count], refs[2 * count:3 * count]
-    isem, osem = refs[3 * count:]
-    incoming, outgoing = [], []
-    slot = 0
-    for src, dst, buf, pieces in zip(sources, targets, held, parts):
+    sources, targets, osem = refs[:count], refs[count:2 * count], refs[2 * count]
+    outgoing = []
+    for src, dst, pieces in zip(sources, targets, parts):
         size = src.shape[0] // pieces
         for p in range(pieces):
             at = pl.ds(p * size, size)
-            incoming.append(pltpu.make_async_copy(src.at[at], buf.at[at], isem.at[slot]))
-            outgoing.append(pltpu.make_async_copy(buf.at[at], dst.at[at], osem.at[slot]))
-            slot += 1
-    for copy in incoming:
+            outgoing.append(pltpu.make_async_copy(src.at[at], dst.at[at], osem.at[len(outgoing)]))
+    for copy in outgoing:
         copy.start()
-    for copy, after in zip(incoming, outgoing):
-        copy.wait()
-        after.start()
     for copy in outgoing:
         copy.wait()
 
 
 def finish(*arrays):
     parts = [4 if a.shape[0] % 128 == 0 else 1 for a in arrays]
-    sems = pltpu.SemaphoreType.DMA((sum(parts),))
     return pl.pallas_call(
         functools.partial(finish_kernel, parts),
         out_shape=[jax.ShapeDtypeStruct(a.shape, a.dtype) for a in arrays],
-        in_specs=[pl.BlockSpec(memory_space=pl.ANY)] * len(arrays),
+        in_specs=[pl.BlockSpec(memory_space=pltpu.VMEM)] * len(arrays),
         out_specs=[pl.BlockSpec(memory_space=pl.ANY)] * len(arrays),
-        scratch_shapes=[pltpu.VMEM(a.shape, a.dtype) for a in arrays] + [sems, sems],
-        compiler_params=pltpu.CompilerParams(vmem_limit_bytes=60 * 1024 * 1024),
-    )(*arrays)
+        scratch_shapes=[pltpu.SemaphoreType.DMA((sum(parts),))],
+    )(*[pltpu.with_memory_space_constraint(a, pltpu.VMEM) for a in arrays])
 
 
 def per_device(value, gate, conv_taps, norm_gain, point_weight, out_grad):
@@ -614,23 +618,22 @@
     units = (peers - 1) * owned
     gain = norm_gain.reshape(1, chans)
     args = (value, gate, conv_taps, gain, point_weight, out_grad)
-    half = (tiles // 2, kw + 1, LANE)
+    piece = (tiles, (kw + 1) // 4, LANE)
     vmem, dma = pltpu.VMEM, pltpu.SemaphoreType.DMA
     block = (SEG, LANE)
     outs = [((rows, chans), BF16), ((rows, chans), BF16), ((kw, chans), F32), ((1, chans), F32), ((per, chans), F32)]
     vgrad, ggrad, taps_grad, gain_grad, wgrad = pl.pallas_call(
         functools.partial(whole_kernel, n, peers),
-        out_shape=[jax.ShapeDtypeStruct(s, d) for s, d in outs],
+        out_shape=[vmem(s, d) for s, d in outs],
         in_specs=[pl.BlockSpec(memory_space=pl.ANY)] * 6,
-        out_specs=[pl.BlockSpec(memory_space=m) for m in (pl.ANY, pl.ANY, vmem, vmem, vmem)],
+        out_specs=[pl.BlockSpec(memory_space=vmem)] * len(outs),
         scratch_shapes=[
             vmem((rows, chans), BF16), vmem((rows, chans), BF16), vmem((full, chans), BF16), vmem((rows, chans), BF16),
             vmem((kw, chans), BF16), vmem((1, chans), F32),
-            vmem((rows, chans), BF16), vmem((rows, chans), BF16),
             vmem((tiles, kw, LANE), F32),
             vmem((tiles, kw) + block, BF16),
             vmem((tiles, kw, 8, LANE), F32),
-            dma((6,)), dma((2, chunks)),
+            dma((6,)),
             vmem((tiles, rows + 4 * EDGE, LANE), F32),
             vmem((tiles, chunks, TAU + kw - 1) + block, BF16),
             vmem((kw + 1,) + block, BF16),
@@ -654,19 +657,18 @@
             vmem((n // 4, per, chans), BF16),
             vmem((group - 1, per, chans), BF16),
             vmem((group - 1, per, chans), BF16),
-            vmem(half, F32),
-            vmem(half, BF16),
-            vmem(half, BF16),
-            vmem((2,) + half, F32),
-            vmem(half, BF16),
-            vmem((group,) + half, BF16),
+            vmem((4,) + piece, BF16),
+            vmem((3,) + piece, BF16),
+            vmem((4,) + piece, F32),
+            vmem(piece, BF16),
+            vmem((group,) + piece, BF16),
             dma((2, 2)), dma((2, 2)), dma((2, peers)), dma((2, peers)),
             dma((units, chunks)), dma((units, chunks)),
             dma((2, peers * owned)), dma((2, peers * owned)), dma((group - 1,)), dma((group - 1,)),
-            dma((3,)), dma((3,)), dma((group - 1,)), dma((group - 1,)),
+            dma((2, 3)), dma((2, 3)), dma((group - 1,)), dma((group - 1,)),
         ],
         compiler_params=pltpu.CompilerParams(
-            collective_id=0, has_side_effects=True, vmem_limit_bytes=60 * 1024 * 1024),
+            collective_id=0, has_side_effects=True, vmem_limit_bytes=52 * 1024 * 1024),
     )(*args)
     vgrad, ggrad, taps_grad, gain_grad, wgrad = finish(vgrad, ggrad, taps_grad, gain_grad, wgrad)
     return vgrad, ggrad, taps_grad, gain_grad.reshape(chans), wgrad

time: 46.3 us -> 43.8 us (0.946)
  the two profiles are of different devices: /device:TPU:5 before, /device:TPU:0 now
where the time goes in v2:
time: 43.8 us; the launch traced here: 43.7 us
  Pallas kernels  43 us (98%)
  between operations  0.64 us (1%)
    pallas_call x1, Pallas kernels, per_device(): pl.pallas_call(functools.partial(whole_kernel, n, peers), out_shape=[vmem...  41.6 us
    pallas_call x1, Pallas kernels, finish(): pl.pallas_call(functools.partial(finish_kernel, parts), out_shape=[jax.Sh...  1.47 us

profile of v2, /device:TPU:0, one launch (start us, length us, event | category | flops | bytes accessed | tf_op | source)
XLA Modules:
  0.0 43.7 jit_solution(3618249757783871259)
XLA Ops:
  0.6 41.6 %shard_map.101 = (bf16[1024,512]{1,0:T(8,128)(2,1)S(1)}, bf16[1024,512]{1,0:T(8,128)(2,1)S(1)}, f32[31,512]{1,0:T(8,128)S(1)}, f32[1,512]{1,0:T(1,128)S(1)}, f32[64,512]{1,0:T(8,128)S(1)}) custom-call(bf16[1024,512]{1,0:T(8,128)(2,1)} %value_in.1, bf16[1024,512]{1,0:T(8,128)(2,1)} %gate_in.1, bf16[31,512]{1,0:T(8,128)(2,1)} %taps_in.1, f32[1,512]{1,0:T(1,128)} %bitcast.2, ...), custom_call_target="tpu_custom_call" | custom-call | tf_op jit(solution)/shard_map/pallas_call | solution.py:625
  42.2 1.5 %shard_map.102 = (bf16[1024,512]{1,0:T(8,128)(2,1)}, bf16[1024,512]{1,0:T(8,128)(2,1)}, f32[31,512]{1,0:T(8,128)}, f32[1,512]{1,0:T(1,128)}, f32[64,512]{1,0:T(8,128)}) custom-call(bf16[1024,512]{1,0:T(8,128)(2,1)S(1)} %get-tuple-element.15.refs_0_, bf16[1024,512]{1,0:T(8,128)(2,1)S(1)} %get-tuple-element.16.refs_1_, ...), custom_call_target="tpu_custom_call" | custom-call | tf_op jit(solution)/shard_map/pallas_call | solution.py:598

commit v3 on v2

--- a/solution.py
+++ b/solution.py
@@ -30,21 +30,23 @@
     return total
 
 
-def group_matrix():
-    row = lax.broadcasted_iota(jnp.int32, (2 * LANE, LANE), 0)
-    col = lax.broadcasted_iota(jnp.int32, (2 * LANE, LANE), 1)
-    same = lax.rem(row, LANE) // GROUP == col // GROUP
-    return jnp.where(same, 1.0 / GROUP, 0.0).astype(BF16)
-
-
-def group_mean(x, matrix):
+def group_matrix(stacked):
+    row = lax.broadcasted_iota(jnp.int32, (2 * LANE, 2 * LANE), 0)
+    col = lax.broadcasted_iota(jnp.int32, (2 * LANE, 2 * LANE), 1)
+    if stacked:
+        row, col = lax.rem(row, LANE), lax.rem(col, LANE)
+    return jnp.where(row // GROUP == col // GROUP, 1.0 / GROUP, 0.0).astype(BF16)
+
+
+def group_mean(x, stacked):
     high = x.astype(BF16)
     low = (x - high.astype(F32)).astype(BF16)
-    return jnp.dot(jnp.concatenate([high, low], axis=1), matrix, preferred_element_type=F32)
-
-
-def near_mean(x, matrix):
-    return jnp.dot(x.astype(BF16), matrix[:LANE], preferred_element_type=F32)
+    return jnp.dot(jnp.concatenate([high, low], axis=1), stacked[:, :LANE], preferred_element_type=F32)
+
+
+def near_means(x, y, apart):
+    both = jnp.dot(jnp.concatenate([x.astype(BF16), y.astype(BF16)], axis=1), apart, preferred_element_type=F32)
+    return both[:, :LANE], both[:, LANE:]
 
 
 def lanes(c):
@@ -91,30 +93,27 @@
             put(first + a, total)
 
 
-def act_to_conv(ng, at, n, own, unit, inv, gain, dconv, gain_part, matrix):
+def act_to_conv(ng, at, n, own, unit, inv, slope, gain, dconv, gain_part, apart):
     for c in range(unit.shape[0]):
         g = gain[:, c * LANE:(c + 1) * LANE]
         u = unit[c, pl.ds(at, n), :]
-        p = u * g
-        s = sigmoid(p)
-        a = ng[:, c * LANE:(c + 1) * LANE] * s * (1.0 + p * (1.0 - s))
+        a = ng[:, c * LANE:(c + 1) * LANE] * slope[c, pl.ds(at, n), :]
         au = a * u
         if own:
             gain_part[:, c * LANE:(c + 1) * LANE] += jnp.sum(au.reshape(n // 8, 8, LANE), axis=0)
         h = a * g
-        hu = au * g
-        dconv[c, pl.ds(at, n), :] = inv[c, pl.ds(at, n), :] * (
-            h - near_mean(h, matrix) - u * near_mean(hu, matrix))
+        first, second = near_means(h, au * g, apart)
+        dconv[c, pl.ds(at, n), :] = inv[c, pl.ds(at, n), :] * (h - first - u * second)
 
 
 def whole_kernel(n, peers, value_in, gate_in, taps_in, gain_in, weight_in, grad_in,
                  vgrad, ggrad, taps_out, gain_out, wout,
-                 value, gate, weight, grad, taps_raw, gain, taps, tapb, tacc, lsem,
-                 gated, shifted, edges, unit, inv, normed, dconv, dshift, dpack, grow, ngacc,
+                 value, gate, weight, grad, taps_raw, gain, taps, tapb, tacc,
+                 gated, shifted, edges, unit, inv, slope, normed, dconv, dshift, dpack, grow, ngacc,
                  gain_part, wpart, sums,
                  vhalo, ohalo, others, send1, recv1, send2, recv2, send3, recv3,
                  asend, arecv, atotal, zsend, zrecv,
-                 vs, vr, os_, or_, gs, gr, ws, wr, ws3, wr3, as_, ar, as3, ar3):
+                 lsem, vs, vr, os_, or_, gs, gr, ws, wr, ws3, wr3, as_, ar, as3, ar3):
     rows, chans = value.shape
     tiles = chans // LANE
     kw = taps.shape[1]
@@ -207,9 +206,8 @@
     for p in range(units):
         for r in range(chunks):
             gather(p, r).start()
-    start_halos(ohalos)
-
-    matrix = group_matrix()
+
+    stacked, apart = group_matrix(True), group_matrix(False)
     loads[3].wait()
     for c in range(tiles):
         taps[c] = taps_raw[:, c * LANE:(c + 1) * LANE].astype(F32)
@@ -289,27 +287,29 @@
     loop(0, tiles, forward_edges)
     loads[4].wait()
 
-    def norm_rows(at, count):
+    def norm_rows(at, count, own):
         xs = [unit[c, pl.ds(at, count), :] for c in range(tiles)]
-        centred = [x - group_mean(x, matrix) for x in xs]
-        out = []
-        for c in range(tiles):
-            rs = lax.rsqrt(near_mean(centred[c] * centred[c], matrix) + EPS)
-            inv[c, pl.ds(at, count), :] = rs
-            u = centred[c] * rs
-            unit[c, pl.ds(at, count), :] = u
-            out.append(u)
-        return out
+        centred = [x - group_mean(x, stacked) for x in xs]
+        for c in range(0, tiles, 2):
+            spreads = near_means(centred[c] * centred[c], centred[c + 1] * centred[c + 1], apart)
+            for e, var in zip((c, c + 1), spreads):
+                rs = lax.rsqrt(var + EPS)
+                inv[e, pl.ds(at, count), :] = rs
+                u = centred[e] * rs
+                unit[e, pl.ds(at, count), :] = u
+                p = u * gain[:, e * LANE:(e + 1) * LANE]
+                s = sigmoid(p)
+                slope[e, pl.ds(at, count), :] = s * (1.0 + p * (1.0 - s))
+                if own is not None:
+                    normed[pl.ds(own, count), e * LANE:(e + 1) * LANE] = (p * s).astype(BF16)
 
     def norm(r):
         at = pl.multiple_of(r * CHUNK, CHUNK)
-        for c, u in enumerate(norm_rows(pl.multiple_of(at + EDGE, 8), CHUNK)):
-            p = u * gain[:, c * LANE:(c + 1) * LANE]
-            normed[pl.ds(at, CHUNK), c * LANE:(c + 1) * LANE] = (p * sigmoid(p)).astype(BF16)
+        norm_rows(pl.multiple_of(at + EDGE, 8), CHUNK, at)
 
     loop(0, chunks, norm)
-    norm_rows(0, EDGE)
-    norm_rows(rows + EDGE, EDGE)
+    norm_rows(0, EDGE, None)
+    norm_rows(rows + EDGE, EDGE, None)
     nstep = divisor(rows, 256, 32)
 
     def owner(j):
@@ -337,10 +337,15 @@
         k = j * owned + p
         return remote(send1.at[at], recv1.at[at], ws.at[0, k], wr.at[0, k], (mate0, tp))
 
-    def half2(j, p):
-        at = pl.ds(unit_of(j, p)[1] // 4, quads)
+    half = chans // 2
+
+    def cols(h):
+        return pl.ds(h * half, half)
+
+    def half2(j, p, h):
+        at = (pl.ds(unit_of(j, p)[1] // 4, quads), slice(None), cols(h))
         k = j * owned + p
-        return remote(send2.at[at], recv2.at[at], ws.at[1, k], wr.at[1, k], (mate1, tp))
+        return remote(send2.at[at], recv2.at[at], ws.at[1 + h, k], wr.at[1 + h, k], (mate1, tp))
 
     def start1(j, p):
         first = unit_of(j, p)[1] // 2
@@ -354,24 +359,31 @@
     def start2(j, p):
         first = unit_of(j, p)[1] // 4
         half1(j, p).wait_recv()
-
-        def cast(i):
-            other, mine = 2 * (first + i) + 1 - b1, 2 * (first + i) + b1
-            send2[first + i] = (wpart[2 * other + b0] + recv1[other].astype(F32)).astype(BF16)
+        for h in range(2):
+            def cast(i, h=h):
+                other = 2 * (first + i) + 1 - b1
+                send2[first + i, :, cols(h)] = (
+                    wpart[2 * other + b0, :, cols(h)] + recv1[other, :, cols(h)].astype(F32)).astype(BF16)
+
+            loop(0, quads, cast)
+            half2(j, p, h).start()
+
+        def keep(i):
+            mine = 2 * (first + i) + b1
             wpart[2 * mine + b0] = wpart[2 * mine + b0] + recv1[mine].astype(F32)
 
-        loop(0, quads, cast)
-        half2(j, p).start()
-
-    def total2(z):
-        return wpart[4 * z + 2 * b1 + b0] + recv2[z].astype(F32)
-
-    def final_copy(slot):
-        return remote(send3.at[slot], recv3.at[slot], ws3.at[slot], wr3.at[slot],
+        loop(0, quads, keep)
+
+    def total2(z, h):
+        return wpart[4 * z + 2 * b1 + b0, :, cols(h)] + recv2[z, :, cols(h)].astype(F32)
+
+    def final_copy(slot, h):
+        at = (slot, slice(None), cols(h))
+        return remote(send3.at[at], recv3.at[at], ws3.at[h, slot], wr3.at[h, slot],
                       (lax.rem(sp + 4 * (slot + 1), n), tp))
 
-    def start3(j, p):
-        half2(j, p).wait_recv()
+    def start3(j, p, h):
+        half2(j, p, h).wait_recv()
         first = unit_of(j, p)[1] // 4
 
         def one(i):
@@ -380,8 +392,8 @@
 
             @pl.when(d != 0)
             def _():
-                send3[d - 1] = total2(z).astype(BF16)
-                final_copy(d - 1).start()
+                send3[d - 1, :, cols(h)] = total2(z, h).astype(BF16)
+                final_copy(d - 1, h).start()
 
         loop(0, far, one)
 
@@ -403,23 +415,22 @@
 
         loop(0, rows // nstep, add)
 
-    last_lane = unit_lane_from(units - 1)
-
     def middle(r):
         at = pl.ds(pl.multiple_of(r * CHUNK, CHUNK), CHUNK)
-        ng = ngacc[at, :] + jnp.dot(others[peers - 2, at, pl.ds(last_lane, UNIT)], weight[weight_rows(peers - 1, last_lane), :],
+        ng = ngacc[at, :] + jnp.dot(others[peers - 2, at, :], weight[pl.ds(pl.multiple_of(owner(peers - 1) * chans, UNIT), chans), :],
                                     preferred_element_type=F32)
-        act_to_conv(ng, pl.multiple_of(r * CHUNK + EDGE, 8), CHUNK, True, unit, inv, gain, dconv, gain_part, matrix)
-
-    def taps_chunk(r):
+        act_to_conv(ng, pl.multiple_of(r * CHUNK + EDGE, 8), CHUNK, True, unit, inv, slope, gain, dconv, gain_part, apart)
+
+    def taps_chunks(*rs):
         def tile(c):
-            for tau in range(TAU):
-                low = r * CHUNK + (EDGE + tau)
-                dpack[c, tau] = spread(dconv, c, low, low + TAU * (SEG // 2), TAU)
+            for i, r in enumerate(rs):
+                for tau in range(TAU):
+                    low = r * CHUNK + (EDGE + tau)
+                    dpack[c, i * TAU + tau] = spread(dconv, c, low, low + TAU * (SEG // 2), TAU)
             for k0 in range(0, kw, 4):
                 ks = range(k0, min(k0 + 4, kw))
-                pairs_ = [[((lambda j=tau + k: shifted[c, r, j]), (lambda tau=tau: dpack[c, tau])) for tau in range(TAU)]
-                          for k in ks]
+                pairs_ = [[((lambda r=r, j=tau + k: shifted[c, r, j]), (lambda i=i, tau=tau: dpack[c, i * TAU + tau]))
+                           for i, r in enumerate(rs) for tau in range(TAU)] for k in ks]
                 for k, total in zip(ks, products(pairs_)):
                     tacc[c, k] += total[:SEG // 2] + total[SEG // 2:]
 
@@ -428,7 +439,11 @@
     def finalize(r):
         gather(units - 1, r).wait_recv()
         middle(r)
-        taps_chunk(r)
+
+    def finalize_two(i):
+        finalize(2 * i)
+        finalize(2 * i + 1)
+        taps_chunks(2 * i, 2 * i + 1)
 
     def fold_taps(c):
         for k in range(kw):
@@ -443,7 +458,7 @@
                     copy.wait_recv()
                 ng = sum(jnp.dot(ohalo[side, j], weight[pl.ds(pl.multiple_of(owner(j) * chans, UNIT), chans), :],
                                  preferred_element_type=F32) for j in range(peers))
-                act_to_conv(ng, at, EDGE, False, unit, inv, gain, dconv, gain_part, matrix)
+                act_to_conv(ng, at, EDGE, False, unit, inv, slope, gain, dconv, gain_part, apart)
 
             @pl.when(jnp.logical_not(arrives[side]))
             def _(at=at):
@@ -499,23 +514,28 @@
             gather(p, r).wait_recv()
         weight_part(p // owned + 1, p % owned, 0, rows, False)
         start1(p // owned + 1, p % owned)
-        unit_ng(p)
+        if p < units - owned:
+            unit_ng(p)
     for p in range(owned):
-        start3(0, p)
+        for h in range(2):
+            start3(0, p, h)
     for p in range(units - 1):
         start2(p // owned + 1, p % owned)
     lj, lp = peers - 1, owned - 1
-    loop(0, 3, finalize)
+    loop(0, 2, finalize_two)
     for p in range(units - 1):
-        start3(p // owned + 1, p % owned)
-    loop(3, chunks - 2, finalize)
+        for h in range(2):
+            start3(p // owned + 1, p % owned, h)
+    loop(2, chunks // 2 - 1, finalize_two)
     weight_part(lj, lp, 0, rows - 2 * CHUNK, False)
     finalize(chunks - 2)
+    taps_chunks(chunks - 2)
     gather(units - 1, chunks - 1).wait_recv()
+    start_halos(ohalos)
     weight_part(lj, lp, rows - 2 * CHUNK, 2 * CHUNK, True)
     start1(lj, lp)
     middle(chunks - 1)
-    taps_chunk(chunks - 1)
+    taps_chunks(chunks - 1)
     loop(0, tiles, fold_taps)
     for q in range(4):
         asend[q] = sums[:, q * part:(q + 1) * part, :].astype(BF16)
@@ -534,11 +554,11 @@
         copy = remote(zsend, zrecv.at[zz], as3.at[d - 1], ar3.at[d - 1], (zmate(d), tp))
         copy.start()
         acopies3.append(copy)
+    loop(5, chunks - 1, backward)
+    start3(lj, lp, 0)
     edge_conv()
-    backward(0)
-    backward(chunks - 1)
-    start3(lj, lp)
-    loop(5, chunks - 1, backward)
+    start3(lj, lp, 1)
+    loop(0, 2, lambda i: backward(i * (chunks - 1)))
     zrecv[zz] = zsend[...]
     for d in range(1, group):
         peer = lax.rem(zz + group - d, group)
@@ -549,11 +569,12 @@
     atotal[quarter] = total
     for d in range(1, 4):
         share(d).start()
-    final = total2(zz)
-    for d in range(1, group):
-        final_copy(d - 1).wait_recv()
-        final += recv3[d - 1].astype(F32)
-    wout[...] = final
+    for h in range(2):
+        final = total2(zz, h)
+        for d in range(1, group):
+            final_copy(d - 1, h).wait_recv()
+            final += recv3[d - 1, :, cols(h)].astype(F32)
+        wout[:, cols(h)] = final
     for d in range(1, 4):
         shared_from(d).wait_recv()
     for c in range(tiles):
@@ -573,24 +594,30 @@
     for j in range(peers):
         for p in range(owned):
             half1(j, p).wait_send()
-            half2(j, p).wait_send()
+            for h in range(2):
+                half2(j, p, h).wait_send()
     for d in range(1, group):
-        final_copy(d - 1).wait_send()
+        for h in range(2):
+            final_copy(d - 1, h).wait_send()
 
 
 def finish_kernel(parts, *refs):
     count = len(parts)
-    sources, targets, osem = refs[:count], refs[count:2 * count], refs[2 * count]
-    outgoing = []
-    for src, dst, pieces in zip(sources, targets, parts):
-        size = src.shape[0] // pieces
-        for p in range(pieces):
-            at = pl.ds(p * size, size)
-            outgoing.append(pltpu.make_async_copy(src.at[at], dst.at[at], osem.at[len(outgoing)]))
-    for copy in outgoing:
-        copy.start()
-    for copy in outgoing:
-        copy.wait()
+    sources, targets = refs[:count], refs[count:]
+
+    def move(osem):
+        outgoing = []
+        for src, dst, pieces in zip(sources, targets, parts):
+            size = src.shape[0] // pieces
+            for p in range(pieces):
+                at = pl.ds(p * size, size)
+                outgoing.append(pltpu.make_async_copy(src.at[at], dst.at[at], osem.at[len(outgoing)]))
+        for copy in outgoing:
+            copy.start()
+        for copy in outgoing:
+            copy.wait()
+
+    pl.run_scoped(move, pltpu.SemaphoreType.DMA((sum(parts),)))
 
 
 def finish(*arrays):
@@ -600,7 +627,6 @@
         out_shape=[jax.ShapeDtypeStruct(a.shape, a.dtype) for a in arrays],
         in_specs=[pl.BlockSpec(memory_space=pltpu.VMEM)] * len(arrays),
         out_specs=[pl.BlockSpec(memory_space=pl.ANY)] * len(arrays),
-        scratch_shapes=[pltpu.SemaphoreType.DMA((sum(parts),))],
     )(*[pltpu.with_memory_space_constraint(a, pltpu.VMEM) for a in arrays])
 
 
@@ -622,8 +648,19 @@
     vmem, dma = pltpu.VMEM, pltpu.SemaphoreType.DMA
     block = (SEG, LANE)
     outs = [((rows, chans), BF16), ((rows, chans), BF16), ((kw, chans), F32), ((1, chans), F32), ((per, chans), F32)]
+    semaphores = [
+            dma((6,)),
+            dma((2, 2)), dma((2, 2)), dma((2, peers)), dma((2, peers)),
+            dma((units, chunks)), dma((units, chunks)),
+            dma((3, peers * owned)), dma((3, peers * owned)), dma((2, group - 1)), dma((2, group - 1)),
+            dma((2, 3)), dma((2, 3)), dma((group - 1,)), dma((group - 1,)),
+    ]
+
+    def scoped_kernel(*refs):
+        pl.run_scoped(lambda *held: whole_kernel(n, peers, *refs, *held), *semaphores)
+
     vgrad, ggrad, taps_grad, gain_grad, wgrad = pl.pallas_call(
-        functools.partial(whole_kernel, n, peers),
+        scoped_kernel,
         out_shape=[vmem(s, d) for s, d in outs],
         in_specs=[pl.BlockSpec(memory_space=pl.ANY)] * 6,
         out_specs=[pl.BlockSpec(memory_space=vmem)] * len(outs),
@@ -633,16 +670,16 @@
             vmem((tiles, kw, LANE), F32),
             vmem((tiles, kw) + block, BF16),
             vmem((tiles, kw, 8, LANE), F32),
-            dma((6,)),
             vmem((tiles, rows + 4 * EDGE, LANE), F32),
             vmem((tiles, chunks, TAU + kw - 1) + block, BF16),
             vmem((kw + 1,) + block, BF16),
             vmem((tiles, extent, LANE), F32),
             vmem((tiles, extent, LANE), F32),
+            vmem((tiles, extent, LANE), F32),
             vmem((rows, chans), BF16),
             vmem((tiles, extent, LANE), F32),
             vmem((TAU + kw - 1,) + block, BF16),
-            vmem((tiles, TAU) + block, BF16),
+            vmem((tiles, 2 * TAU) + block, BF16),
             vmem((tiles, CHUNK, LANE), F32),
             vmem((rows, chans), F32),
             vmem((8, chans), F32),
@@ -662,10 +699,6 @@
             vmem((4,) + piece, F32),
             vmem(piece, BF16),
             vmem((group,) + piece, BF16),
-            dma((2, 2)), dma((2, 2)), dma((2, peers)), dma((2, peers)),
-            dma((units, chunks)), dma((units, chunks)),
-            dma((2, peers * owned)), dma((2, peers * owned)), dma((group - 1,)), dma((group - 1,)),
-            dma((2, 3)), dma((2, 3)), dma((group - 1,)), dma((group - 1,)),
         ],
         compiler_params=pltpu.CompilerParams(
             collective_id=0, has_side_effects=True, vmem_limit_bytes=52 * 1024 * 1024),

time: 43.8 us -> 42.4 us (0.968)
  Pallas kernels: 43 us -> 41.6 us
    pallas_call x1, Pallas kernels: 41.6 us -> 40.2 us  [per_device(): pl.pallas_call(scoped_kernel, out_shape=[vmem(s, d) for s, d in outs], in...]
where the time goes in v3:
time: 42.4 us; the launch traced here: 42.3 us
  Pallas kernels  41.6 us (98%)
  between operations  0.64 us (2%)
    pallas_call x1, Pallas kernels, per_device(): pl.pallas_call(scoped_kernel, out_shape=[vmem(s, d) for s, d in outs], in...  40.2 us
    pallas_call x1, Pallas kernels, finish(): pl.pallas_call(functools.partial(finish_kernel, parts), out_shape=[jax.Sh...  1.37 us

profile of v3, /device:TPU:0, one launch (start us, length us, event | category | flops | bytes accessed | tf_op | source)
XLA Modules:
  0.0 42.3 jit_solution(8619459646323857589)
XLA Ops:
  0.6 40.2 %shard_map.101 = (bf16[1024,512]{1,0:T(8,128)(2,1)S(1)}, bf16[1024,512]{1,0:T(8,128)(2,1)S(1)}, f32[31,512]{1,0:T(8,128)S(1)}, f32[1,512]{1,0:T(1,128)S(1)}, f32[64,512]{1,0:T(8,128)S(1)}) custom-call(bf16[1024,512]{1,0:T(8,128)(2,1)} %refs_0_.1, bf16[1024,512]{1,0:T(8,128)(2,1)} %refs_1_.1, bf16[31,512]{1,0:T(8,128)(2,1)} %refs_2_.1, f32[1,512]{1,0:T(1,128)} %bitcast.2, ...), custom_call_target="tpu_custom_call" | custom-call | tf_op jit(solution)/shard_map/pallas_call | solution.py:662
  40.9 1.4 %shard_map.102 = (bf16[1024,512]{1,0:T(8,128)(2,1)}, bf16[1024,512]{1,0:T(8,128)(2,1)}, f32[31,512]{1,0:T(8,128)}, f32[1,512]{1,0:T(1,128)}, f32[64,512]{1,0:T(8,128)}) custom-call(bf16[1024,512]{1,0:T(8,128)(2,1)S(1)} %get-tuple-element.15.refs_0_, bf16[1024,512]{1,0:T(8,128)(2,1)S(1)} %get-tuple-element.16.refs_1_, ...), custom_call_target="tpu_custom_call" | custom-call | tf_op jit(solution)/shard_map/pallas_call | solution.py:625

commit v4 on v3

--- a/solution.py
+++ b/solution.py
@@ -487,19 +487,26 @@
 
         loop(0, tiles, tile)
 
-    part = (kw + 1) // 4
-
-    def slot(d):
+    part = (kw + 1) // 2
+    collects = b0 == 1
+
+    def collector(q):
+        return sp - quarter + 2 * q + 1
+
+    def gather_sums(q, sender):
+        return remote(asend.at[q], arecv.at[sender], as_.at[0, q], ar.at[0, sender], (collector(q), tp))
+
+    def other(d):
         return lax.rem(quarter + d, 4)
 
-    def gather_sums(d):
-        return remote(asend.at[slot(d)], arecv.at[d - 1], as_.at[0, d - 1], ar.at[0, d - 1], (plane(d), tp))
-
     def share(d):
-        return remote(atotal.at[quarter], atotal.at[quarter], as_.at[1, d - 1], ar.at[1, d - 1], (plane(d), tp))
-
-    def shared_from(d):
-        return remote(atotal.at[slot(4 - d)], atotal.at[slot(4 - d)], as_.at[1, d - 1], ar.at[1, d - 1], (plane(d), tp))
+        return remote(atotal.at[b1], atotal.at[b1], as_.at[1, d - 1], ar.at[1, b1], (plane(d), tp))
+
+    def spread_sums(d):
+        return remote(zsend, zrecv.at[zz], as3.at[d - 1], ar3.at[d - 1], (zmate(d), tp))
+
+    def shared(q):
+        return remote(atotal.at[q], atotal.at[q], as_.at[1, 0], ar.at[1, q], (plane(1), tp))
 
     loads[2].wait()
     for p in range(owned):
@@ -531,63 +538,86 @@
     finalize(chunks - 2)
     taps_chunks(chunks - 2)
     gather(units - 1, chunks - 1).wait_recv()
+    middle(chunks - 1)
+    taps_chunks(chunks - 1)
+    loop(0, tiles, fold_taps)
+    for q in range(2):
+        asend[q] = sums[:, q * part:(q + 1) * part, :].astype(BF16)
+
+        @pl.when(quarter != 2 * q + 1)
+        def _(q=q):
+            gather_sums(q, quarter).start()
+
     start_halos(ohalos)
     weight_part(lj, lp, rows - 2 * CHUNK, 2 * CHUNK, True)
     start1(lj, lp)
-    middle(chunks - 1)
-    taps_chunks(chunks - 1)
-    loop(0, tiles, fold_taps)
-    for q in range(4):
-        asend[q] = sums[:, q * part:(q + 1) * part, :].astype(BF16)
-    for d in range(1, 4):
-        gather_sums(d).start()
+    loop(1, 3, backward)
     start2(lj, lp)
-    loop(1, 5, backward)
-    for d in range(1, 4):
-        gather_sums(d).wait_recv()
-    mine = sums[:, pl.ds(pl.multiple_of(quarter * part, part), part), :]
-    for d in range(3):
-        mine += arecv[d].astype(F32)
-    zsend[...] = mine.astype(BF16)
-    acopies3 = []
-    for d in range(1, group):
-        copy = remote(zsend, zrecv.at[zz], as3.at[d - 1], ar3.at[d - 1], (zmate(d), tp))
-        copy.start()
-        acopies3.append(copy)
-    loop(5, chunks - 1, backward)
+    backward(3)
+
+    @pl.when(collects)
+    def _():
+        for d in range(1, 4):
+            gather_sums(0, other(d)).wait_recv()
+        mine = sums[:, pl.ds(pl.multiple_of(b1 * part, part), part), :]
+        for d in range(1, 4):
+            mine += arecv[other(d)].astype(F32)
+        zsend[...] = mine.astype(BF16)
+        for d in range(1, group):
+            spread_sums(d).start()
+
+    loop(4, chunks - 1, backward)
+    edge_conv()
     start3(lj, lp, 0)
-    edge_conv()
+    backward(0)
     start3(lj, lp, 1)
-    loop(0, 2, lambda i: backward(i * (chunks - 1)))
-    zrecv[zz] = zsend[...]
-    for d in range(1, group):
-        peer = lax.rem(zz + group - d, group)
-        remote(zsend, zrecv.at[peer], as3.at[d - 1], ar3.at[d - 1], (zmate(d), tp)).wait_recv()
-    total = zrecv[0].astype(F32)
-    for z in range(1, group):
-        total += zrecv[z].astype(F32)
-    atotal[quarter] = total
-    for d in range(1, 4):
-        share(d).start()
+
+    @pl.when(collects)
+    def _():
+        zrecv[zz] = zsend[...]
+        for d in range(1, group):
+            peer = lax.rem(zz + group - d, group)
+            remote(zsend, zrecv.at[peer], as3.at[d - 1], ar3.at[d - 1], (zmate(d), tp)).wait_recv()
+        total = zrecv[0].astype(F32)
+        for z in range(1, group):
+            total += zrecv[z].astype(F32)
+        atotal[b1] = total
+        for d in (1, 3, 2):
+            share(d).start()
+
+    backward(chunks - 1)
     for h in range(2):
         final = total2(zz, h)
         for d in range(1, group):
             final_copy(d - 1, h).wait_recv()
             final += recv3[d - 1, :, cols(h)].astype(F32)
         wout[:, cols(h)] = final
-    for d in range(1, 4):
-        shared_from(d).wait_recv()
+    for q in range(2):
+        @pl.when(quarter != 2 * q + 1)
+        def _(q=q):
+            shared(q).wait_recv()
+
     for c in range(tiles):
-        tot = jnp.concatenate([atotal[q, c] for q in range(4)], axis=0)
+        tot = jnp.concatenate([atotal[q, c] for q in range(2)], axis=0)
         taps_out[:, c * LANE:(c + 1) * LANE] = tot[:kw]
         gain_out[:, c * LANE:(c + 1) * LANE] = tot[kw:]
+    for q in range(2):
+        @pl.when(quarter != 2 * q + 1)
+        def _(q=q):
+            gather_sums(q, quarter).wait_send()
+
+    @pl.when(collects)
+    def _():
+        for d in range(1, 4):
+            share(d).wait_send()
+        for d in range(1, group):
+            spread_sums(d).wait_send()
+
     for side in range(2):
         @pl.when(sends[side])
         def _(side=side):
             for copy in halos[side] + ohalos[side]:
                 copy.wait_send()
-    for copy in acopies3 + [gather_sums(d) for d in range(1, 4)] + [share(d) for d in range(1, 4)]:
-        copy.wait_send()
     for p in range(units):
         for r in range(chunks):
             gather(p, r).wait_send()
@@ -644,7 +674,7 @@
     units = (peers - 1) * owned
     gain = norm_gain.reshape(1, chans)
     args = (value, gate, conv_taps, gain, point_weight, out_grad)
-    piece = (tiles, (kw + 1) // 4, LANE)
+    piece = (tiles, (kw + 1) // 2, LANE)
     vmem, dma = pltpu.VMEM, pltpu.SemaphoreType.DMA
     block = (SEG, LANE)
     outs = [((rows, chans), BF16), ((rows, chans), BF16), ((kw, chans), F32), ((1, chans), F32), ((per, chans), F32)]
@@ -653,7 +683,7 @@
             dma((2, 2)), dma((2, 2)), dma((2, peers)), dma((2, peers)),
             dma((units, chunks)), dma((units, chunks)),
             dma((3, peers * owned)), dma((3, peers * owned)), dma((2, group - 1)), dma((2, group - 1)),
-            dma((2, 3)), dma((2, 3)), dma((group - 1,)), dma((group - 1,)),
+            dma((2, 3)), dma((2, 4)), dma((group - 1,)), dma((group - 1,)),
     ]
 
     def scoped_kernel(*refs):
@@ -694,9 +724,9 @@
             vmem((n // 4, per, chans), BF16),
             vmem((group - 1, per, chans), BF16),
             vmem((group - 1, per, chans), BF16),
+            vmem((2,) + piece, BF16),
             vmem((4,) + piece, BF16),
-            vmem((3,) + piece, BF16),
-            vmem((4,) + piece, F32),
+            vmem((2,) + piece, F32),
             vmem(piece, BF16),
             vmem((group,) + piece, BF16),
         ],

time: 42.4 us -> 40.7 us (0.960)
  Pallas kernels: 41.6 us -> 39.9 us
    pallas_call x1, Pallas kernels: 40.2 us -> 38.6 us  [per_device(): pl.pallas_call(scoped_kernel, out_shape=[vmem(s, d) for s, d in outs], in...]
where the time goes in v4:
time: 40.7 us; the launch traced here: 40.6 us
  Pallas kernels  39.9 us (98%)
  between operations  0.64 us (2%)
    pallas_call x1, Pallas kernels, per_device(): pl.pallas_call(scoped_kernel, out_shape=[vmem(s, d) for s, d in outs], in...  38.6 us
    pallas_call x1, Pallas kernels, finish(): pl.pallas_call(functools.partial(finish_kernel, parts), out_shape=[jax.Sh...  1.37 us

profile of v4, /device:TPU:0, one launch (start us, length us, event | category | flops | bytes accessed | tf_op | source)
XLA Modules:
  0.0 40.6 jit_solution(4080389365254354381)
XLA Ops:
  0.6 38.6 %shard_map.101 = (bf16[1024,512]{1,0:T(8,128)(2,1)S(1)}, bf16[1024,512]{1,0:T(8,128)(2,1)S(1)}, f32[31,512]{1,0:T(8,128)S(1)}, f32[1,512]{1,0:T(1,128)S(1)}, f32[64,512]{1,0:T(8,128)S(1)}) custom-call(bf16[1024,512]{1,0:T(8,128)(2,1)} %refs_0_.1, bf16[1024,512]{1,0:T(8,128)(2,1)} %refs_1_.1, bf16[31,512]{1,0:T(8,128)(2,1)} %refs_2_.1, f32[1,512]{1,0:T(1,128)} %bitcast.2, ...), custom_call_target="tpu_custom_call" | custom-call | tf_op jit(solution)/shard_map/pallas_call | solution.py:692
  39.2 1.4 %shard_map.102 = (bf16[1024,512]{1,0:T(8,128)(2,1)}, bf16[1024,512]{1,0:T(8,128)(2,1)}, f32[31,512]{1,0:T(8,128)}, f32[1,512]{1,0:T(1,128)}, f32[64,512]{1,0:T(8,128)}) custom-call(bf16[1024,512]{1,0:T(8,128)(2,1)S(1)} %get-tuple-element.15.refs_0_, bf16[1024,512]{1,0:T(8,128)(2,1)S(1)} %get-tuple-element.16.refs_1_, ...), custom_call_target="tpu_custom_call" | custom-call | tf_op jit(solution)/shard_map/pallas_call | solution.py:655

commit v5 on v4

--- a/solution.py
+++ b/solution.py
@@ -203,9 +203,17 @@
         return pl.multiple_of(jnp.where(2 * sender < peers, q, owned - 1 - q) * UNIT, UNIT)
 
     start_halos(halos)
+    held = range(chunks - 2, chunks)
+
+    def start_held():
+        for r in held:
+            gather(units - 1, r).start()
+
     for p in range(units):
         for r in range(chunks):
-            gather(p, r).start()
+            if p < units - 1 or r not in held:
+                gather(p, r).start()
+    pl.when(b0 == 0)(start_held)
 
     stacked, apart = group_matrix(True), group_matrix(False)
     loads[3].wait()
@@ -421,7 +429,7 @@
                                     preferred_element_type=F32)
         act_to_conv(ng, pl.multiple_of(r * CHUNK + EDGE, 8), CHUNK, True, unit, inv, slope, gain, dconv, gain_part, apart)
 
-    def taps_chunks(*rs):
+    def taps_chunks(*rs, flat=False):
         def tile(c):
             for i, r in enumerate(rs):
                 for tau in range(TAU):
@@ -434,7 +442,11 @@
                 for k, total in zip(ks, products(pairs_)):
                     tacc[c, k] += total[:SEG // 2] + total[SEG // 2:]
 
-        loop(0, tiles, tile)
+        if flat:
+            for c in range(tiles):
+                tile(c)
+        else:
+            loop(0, tiles, tile)
 
     def finalize(r):
         gather(units - 1, r).wait_recv()
@@ -533,13 +545,18 @@
     for p in range(units - 1):
         for h in range(2):
             start3(p // owned + 1, p % owned, h)
-    loop(2, chunks // 2 - 1, finalize_two)
+    loop(2, chunks // 2 - 2, finalize_two)
+    gather(units - 1, chunks - 4).wait_recv()
+    pl.when(b0 == 1)(start_held)
+    middle(chunks - 4)
+    finalize(chunks - 3)
+    taps_chunks(chunks - 4, chunks - 3)
     weight_part(lj, lp, 0, rows - 2 * CHUNK, False)
     finalize(chunks - 2)
     taps_chunks(chunks - 2)
     gather(units - 1, chunks - 1).wait_recv()
     middle(chunks - 1)
-    taps_chunks(chunks - 1)
+    taps_chunks(chunks - 1, flat=True)
     loop(0, tiles, fold_taps)
     for q in range(2):
         asend[q] = sums[:, q * part:(q + 1) * part, :].astype(BF16)
@@ -567,9 +584,7 @@
             spread_sums(d).start()
 
     loop(4, chunks - 1, backward)
-    edge_conv()
     start3(lj, lp, 0)
-    backward(0)
     start3(lj, lp, 1)
 
     @pl.when(collects)
@@ -585,7 +600,8 @@
         for d in (1, 3, 2):
             share(d).start()
 
-    backward(chunks - 1)
+    edge_conv()
+    loop(0, 2, lambda i: backward(i * (chunks - 1)))
     for h in range(2):
         final = total2(zz, h)
         for d in range(1, group):

time: 40.7 us -> 40.3 us (level)
    pallas_call x1, Pallas kernels: 38.6 us -> 38.1 us  [per_device(): pl.pallas_call(scoped_kernel, out_shape=[vmem(s, d) for s, d in outs], in...]
where the time goes in v5:
time: 40.3 us; the launch traced here: 40.1 us
  Pallas kernels  39.5 us (98%)
  between operations  0.64 us (2%)
    pallas_call x1, Pallas kernels, per_device(): pl.pallas_call(scoped_kernel, out_shape=[vmem(s, d) for s, d in outs], in...  38.1 us
    pallas_call x1, Pallas kernels, finish(): pl.pallas_call(functools.partial(finish_kernel, parts), out_shape=[jax.Sh...  1.37 us

profile of v5, /device:TPU:0, one launch (start us, length us, event | category | flops | bytes accessed | tf_op | source)
XLA Modules:
  0.0 40.1 jit_solution(17291176575406545750)
XLA Ops:
  0.6 38.1 %shard_map.101 = (bf16[1024,512]{1,0:T(8,128)(2,1)S(1)}, bf16[1024,512]{1,0:T(8,128)(2,1)S(1)}, f32[31,512]{1,0:T(8,128)S(1)}, f32[1,512]{1,0:T(1,128)S(1)}, f32[64,512]{1,0:T(8,128)S(1)}) custom-call(bf16[1024,512]{1,0:T(8,128)(2,1)} %refs_0_.1, bf16[1024,512]{1,0:T(8,128)(2,1)} %refs_1_.1, bf16[31,512]{1,0:T(8,128)(2,1)} %refs_2_.1, f32[1,512]{1,0:T(1,128)} %bitcast.2, ...), custom_call_target="tpu_custom_call" | custom-call | tf_op jit(solution)/shard_map/pallas_call | solution.py:708
  38.7 1.4 %shard_map.102 = (bf16[1024,512]{1,0:T(8,128)(2,1)}, bf16[1024,512]{1,0:T(8,128)(2,1)}, f32[31,512]{1,0:T(8,128)}, f32[1,512]{1,0:T(1,128)}, f32[64,512]{1,0:T(8,128)}) custom-call(bf16[1024,512]{1,0:T(8,128)(2,1)S(1)} %get-tuple-element.15.refs_0_, bf16[1024,512]{1,0:T(8,128)(2,1)S(1)} %get-tuple-element.16.refs_1_, ...), custom_call_target="tpu_custom_call" | custom-call | tf_op jit(solution)/shard_map/pallas_call | solution.py:671
